TPU v7x, 256 devices: a whole 4x4x8 slice. The times are simulated.
256 devices in a mesh: sp: 64 (over z, x, core), tp: 4 (over y).
Axes of the slice: x: 4, y: 4, z: 8, core: 2. Of those that a mesh axis runs over, the one named last changes fastest.
Arguments:
- queries: bfloat16 [40960, 2048], P('sp', 'tp'), may hold values from -164 to 164
- keys: bfloat16 [40960, 512], P('sp', 'tp'), may hold values from -6 to 6
- values: bfloat16 [40960, 512], P('sp', 'tp'), may hold values from -6 to 6
- sink: float32 [32], P('tp'), may hold values from 4 to 8
- stream: bfloat16 [40960, 2048], P(('sp', 'tp')), may hold values from -6 to 6
- out_weight: bfloat16 [2048, 2048], P('tp'), may hold values from -0.5390625 to 0.5390625
- norm_gain: float32 [2048], replicated, may hold values from 0.1 to 1.9
- gate_weight: bfloat16 [2048, 5632], P('sp', 'tp'), may hold values from -0.125 to 0.125
- up_weight: bfloat16 [2048, 5632], P('sp', 'tp'), may hold values from -0.125 to 0.125
- down_weight: bfloat16 [5632, 2048], P('tp', 'sp'), may hold values from -0.23925781 to 0.23925781
Outputs:
- result: bfloat16 [40960, 2048], P(('sp', 'tp'))
All inputs are finite; a program needn't handle non-finite values.
Results may differ from a plain program's by a relative error of at most 0.019.
Values may be sent and summed in bfloat16 or wider, within the bound.
A program may use at most 128 MiB of HBM per device.

v0:
```python
import jax
import jax.numpy as jnp
from jax import lax
from jax.sharding import PartitionSpec as P

HEAD = 64
WINDOW = 128


def padded_2(cells, sides, width):
    for axis, dim in sides:
        count = lax.axis_size(axis)
        ends = count - 1
        head = lax.slice_in_dim(cells, 0, width, axis=dim)
        tail = lax.slice_in_dim(cells, cells.shape[dim] - width, cells.shape[dim], axis=dim)
        cells = jnp.concatenate(
            [
                lax.ppermute(tail, axis, [(i, (i + 1) % count) for i in range(ends)]),
                cells,
                lax.ppermute(head, axis, [((i + 1) % count, i) for i in range(ends)]),
            ],
            axis=dim,
        )
    return cells


def rows_first(arrays, axis, dims):
    turned = [jnp.moveaxis(a, dim, 0) for a, dim in zip(arrays, dims)]
    both = jnp.concatenate([t.reshape(len(t), -1) for t in turned], axis=1)
    whole, at, done = (lax.all_gather(both, axis, axis=0, tiled=True), 0, [])
    for t, dim in zip(turned, dims):
        section = whole[:, at : at + t[0].size].reshape(-1, *t.shape[1:])
        done.append(jnp.moveaxis(section, 0, dim))
        at += t[0].size
    return tuple(done)


def in_blocks(value, dim, size):
    dims = value.shape
    tiles = value.reshape(*dims[:dim], size, dims[dim] // size, *dims[dim + 1 :])
    return jnp.moveaxis(tiles, dim, 0)


def sent_and_summed(value, axis, dim):
    tiles = in_blocks(value, dim, lax.axis_size(axis))
    arrived = lax.all_to_all(tiles, axis, split_axis=0, concat_axis=0, tiled=True)
    return arrived.astype(jnp.float32).sum(axis=0)


def copy_for_each(value, axis):
    copies = jnp.broadcast_to(value, (lax.axis_size(axis), *value.shape))
    return lax.all_to_all(copies, axis, split_axis=0, concat_axis=0, tiled=True)


def joined_along(tiles, dim):
    tiles = jnp.moveaxis(tiles, 0, dim)
    dims = tiles.shape
    return tiles.reshape(*dims[:dim], dims[dim] * dims[dim + 1], *dims[dim + 2 :])


def gather_directly(value, axis, dim):
    tiles = copy_for_each(value, axis)
    return joined_along(tiles, dim)


def rotary(block, start):
    length = block.shape[0]
    middle = HEAD // 2
    inverse = 1.0 / 10000.0 ** (jnp.arange(0, HEAD, 2, dtype=jnp.float32) / HEAD)
    places = (start + jnp.arange(length, dtype=jnp.int32)).astype(jnp.float32)
    angles = places[:, None, None] * inverse[None, None, :]
    cosine_table = jnp.cos(angles)
    sine_table = jnp.sin(angles)
    pieces = block.astype(jnp.float32).reshape(length, -1, HEAD)
    leading = pieces[..., :middle]
    trailing = pieces[..., middle:]
    turned = jnp.concatenate(
        [
            leading * cosine_table - trailing * sine_table,
            trailing * cosine_table + leading * sine_table,
        ],
        -1,
    )
    return turned.reshape(length, -1).astype(jnp.bfloat16)


def window_attend(queries, keys, values, sink):
    rows_here = queries.shape[0]
    start = lax.axis_index("sp") * rows_here
    length = lax.axis_size("sp") * rows_here
    blocks = rows_here // WINDOW
    kv_width = keys.shape[1]
    kv_count = kv_width // HEAD
    head_count = queries.shape[1] // HEAD
    group = head_count // kv_count
    turned_q = rotary(queries, start)
    turned_k = rotary(keys, start)
    paired = jnp.concatenate([turned_k, values], 1)
    padded = padded_2(paired, (("sp", 0),), WINDOW)
    framed = padded.reshape(blocks + 2, WINDOW, 2 * kv_width)
    banded = jnp.concatenate([framed[:-2], framed[1:-1], framed[2:]], axis=1)
    key_band = banded[..., :kv_width].reshape(blocks, 3 * WINDOW, kv_count, HEAD)
    value_band = banded[..., kv_width:].reshape(blocks, 3 * WINDOW, kv_count, HEAD)
    query_blocks = turned_q.reshape(blocks, WINDOW, kv_count, group, HEAD)
    scores = jnp.einsum(
        "nqkgd,nskd->nkgqs", query_blocks, key_band, preferred_element_type=jnp.float32
    ) * HEAD ** (-0.5)
    query_place = (
        start + jnp.arange(blocks)[:, None, None] * WINDOW + jnp.arange(WINDOW)[None, :, None]
    )
    key_place = (
        start
        + jnp.arange(blocks)[:, None, None] * WINDOW
        - WINDOW
        + jnp.arange(3 * WINDOW)[None, None, :]
    )
    valid = (jnp.abs(key_place - query_place) <= WINDOW) & (key_place >= 0) & (key_place < length)
    scores = jnp.where(valid[:, None, None], scores, -jnp.inf)
    sink_grid = sink.reshape(kv_count, group)[None, :, :, None]
    top = jnp.maximum(jnp.max(scores, -1), sink_grid)
    raised = jnp.exp(scores - top[..., None])
    denom = jnp.sum(raised, -1) + jnp.exp(sink_grid - top)
    weights = (raised / denom[..., None]).astype(jnp.bfloat16)
    output = jnp.einsum(
        "nkgqs,nskd->nqkgd", weights, value_band, preferred_element_type=jnp.float32
    )
    return output.astype(jnp.bfloat16).reshape(rows_here, head_count * HEAD)


def collect_weights(gate_weight, up_weight, down_weight):
    return rows_first((gate_weight, up_weight, down_weight), "sp", (0, 0, 1))


def local(
    queries, keys, values, sink, stream, out_weight, norm_gain, gate_weight, up_weight, down_weight
):
    attended = window_attend(queries, keys, values, sink)
    gathered = collect_weights(gate_weight, up_weight, down_weight)
    gate_whole, up_whole, down_whole = gathered
    rows = attended
    projected = sent_and_summed(
        jnp.dot(rows, out_weight, preferred_element_type=jnp.float32).astype(jnp.bfloat16), "tp", 0
    )
    mixed = (stream.astype(jnp.float32) + projected).astype(jnp.bfloat16)
    mixed_wide = mixed.astype(jnp.float32)
    scale = lax.rsqrt(jnp.mean(mixed_wide * mixed_wide, -1, keepdims=True) + 1e-06)
    normed = (mixed_wide * scale * norm_gain).astype(jnp.bfloat16)
    piece = gather_directly(normed, "tp", 0)
    gate = jnp.dot(piece, gate_whole, preferred_element_type=jnp.float32)
    upward = jnp.dot(piece, up_whole, preferred_element_type=jnp.float32)
    hidden = (jax.nn.silu(gate) * upward).astype(jnp.bfloat16)
    rows = hidden
    lowered = sent_and_summed(
        jnp.dot(rows, down_whole, preferred_element_type=jnp.float32).astype(jnp.bfloat16), "tp", 0
    )
    return (mixed_wide + 0.5 * lowered).astype(jnp.bfloat16)


def solution(mesh):
    placed = (
        P("sp", "tp"),
        P("sp", "tp"),
        P("sp", "tp"),
        P("tp"),
        P(("sp", "tp"), None),
        P("tp", None),
        P(),
        P("sp", "tp"),
        P("sp", "tp"),
        P("tp", "sp"),
    )
    return jax.shard_map(
        local, mesh=mesh, in_specs=placed, out_specs=P(("sp", "tp"), None), check_vma=False
    )
```

profile of v0, /device:TPU:1, one launch (start us, length us, event | category | flops | bytes accessed | tf_op | source)
XLA Modules:
  0.0 188.8 jit_solution(6762812232061764463)
XLA Ops:
  6.5 0.0 copy-start
  6.5 0.0 all-gather.2.cloned.1.call-start
  6.5 1.8 pad_maximum_fusion.7
  8.4 0.0 all-gather.2.cloned.1.call-update
  8.4 1.1 copy.24
  9.5 1.1 copy.25
  10.6 0.4 multiply_cosine_fusion
  11.1 0.0 copy-start.1
  11.1 0.7 fusion.33
  11.8 4.5 %collective-permute-start = (bf16[128,256]{0,1:T(8,128)(2,1)}, bf16[128,256]{0,1:T(8,128)(2,1)}, u32[]{:S(2)}, u32[]{:S(2)}) collective-permute-start(bf16[128,256]{0,1:T(8,128)(2,1)} %get-tuple-element.16), channel_id=1, source_target_pairs={{0,4},{4,8},{8,12},{12,16},{16,20},{20,24},{24,28},{28,32},{32,36}... | collective-permute-start | bytes 196616 | tf_op jit(solution)/shard_map/ppermute | solution.py:18
  16.3 0.0 copy-done.1
  16.3 2.5 %collective-permute-start.1 = (bf16[128,256]{0,1:T(8,128)(2,1)}, bf16[128,256]{0,1:T(8,128)(2,1)}, u32[]{:S(2)}, u32[]{:S(2)}) collective-permute-start(bf16[128,256]{0,1:T(8,128)(2,1)} %get-tuple-element.17), channel_id=1, source_target_pairs={{4,0},{8,4},{12,8},{16,12},{20,16},{24,20},{28,24},{32,28},{36,32}... | collective-permute-start | bytes 196616 | tf_op jit(solution)/shard_map/ppermute | solution.py:20
  18.8 1.4 copy.31
  20.2 0.1 convert.19
  20.3 0.1 iota_add_fusion.1
  20.4 0.1 fusion.36
  20.4 0.1 iota_add_fusion
  20.5 1.2 fusion.28
  21.7 0.2 subtract_convert_fusion
  21.9 0.9 pad_maximum_fusion.1
  22.8 1.8 convert_element_type.61
  24.6 1.3 max.17
  25.9 0.0 collective-permute-done
  25.9 0.0 collective-permute-done.1
  25.9 2.1 %pad_maximum_fusion.5 = (bf16[640,256]{0,1:T(8,128)(2,1)}, bf16[640,256]{0,1:T(8,128)(2,1)}, bf16[640,256]{0,1:T(8,128)(2,1)}) fusion(bf16[128,256]{0,1:T(8,128)(2,1)} %collective-permute-done, bf16[640,128]{0,1:T(8,128)(2,1)S(1)} %copy.25, bf16[640,128]{0,1:T(8,128)(2,1)} %bitcast.58, bf16[128,256]{0,1:T(8,128)(2,1)} %collective-permute-done.1), kind=kLoop, calls=%fused_computation.47 | loop fusion | flops 2621440 | bytes 1441792 | tf_op jit(solution)/shard_map/concatenate | solution.py:16
  28.0 1.9 copy.26
  29.9 1.9 copy.27
  31.7 1.9 copy.28
  33.6 1.2 pad_maximum_fusion
  34.8 1.2 fusion.40
  36.0 2.0 %copy.30 = bf16[5,384,128]{1,2,0:T(8,128)(2,1)} copy(bf16[5,384,128]{2,1,0:T(8,128)(2,1)} %get-tuple-element.9) | data formatting | bytes 983040 | tf_op jit(solution)/shard_map/slice | solution.py:102
  38.0 2.0 %copy.29 = bf16[5,384,128]{1,2,0:T(8,128)(2,1)} copy(bf16[5,384,128]{2,1,0:T(8,128)(2,1)} %get-tuple-element.10) | data formatting | bytes 983040 | tf_op jit(solution)/shard_map/slice | solution.py:103
  40.1 0.0 copy-start.5
  40.1 2.3 %fusion.1 = (f32[5,2,4,128]{3,2,1,0:T(4,128)S(1)}, f32[5,2,384,128,4]{3,2,4,1,0:T(8,128)S(1)}) fusion(pred[5,128,384]{1,2,0:T(8,128)(4,1)S(1)} %fusion.28, bf16[5,384,2,64,1]{1,3,4,2,0:T(8,128)(2,1)} %bitcast.56, bf16[5,128,2,4,64]{1,0,4,3,2:T(8,128)(2,1)S(1)} %convert_element_type.61), kind=kOutput, calls=%fused_computation.4 | convolution fusion | flops 257551360 | bytes 9277440 | tf_op jit(solution)/shard_map/nqkgd,nskd->nkgqs/dot_general | solution.py:105
  42.4 0.0 copy-done.5
  42.4 0.1 broadcast_maximum_fusion
  42.4 0.0 copy-start.3
  42.4 1.9 %fusion = f32[5,2,4,128]{3,2,1,0:T(4,128)S(1)} fusion(f32[5,2,384,128,4]{3,2,4,1,0:T(8,128)S(1)} %get-tuple-element.23, f32[5,2,4,128]{3,2,1,0:T(4,128)S(1)} %broadcast_maximum_fusion, pred[5,128,384]{1,2,0:T(8,128)(4,1)S(1)} %fusion.28), kind=kLoop, calls=%fused_computation.3 | loop fusion | flops 7859200 | bytes 8151040 | tf_op jit(solution)/shard_map/reduce_sum | solution.py:122
  44.4 0.1 exponential_add_fusion
  44.5 0.0 copy-done.3
  44.5 2.4 %fusion.26 = bf16[5,128,2,4,64]{1,4,3,2,0:T(8,128)(2,1)S(1)} fusion(bf16[5,384,2,64,1]{1,3,4,2,0:T(8,128)(2,1)S(1)} %bitcast.64, f32[5,2,384,128,4]{3,2,4,1,0:T(8,128)S(1)} %get-tuple-element.23, f32[5,2,4,128]{3,2,1,0:T(4,128)S(1)} %exponential_add_fusion, f32[5,2,4,128]{3,2,1,0:T(4,128)S(1)} %broadcast_maximum_fusion, pred[5,128,384]{1,2,0:T(8,128)(4,1)S(1)} %fusion.28), kind=kOutput, calls=%fused_computation.28 | convolution fusion | flops 261816320 | bytes 9297920 | tf_op jit(solution)/shard_map/nkgqs,nskd->nqkgd/dot_general | solution.py:124
  46.8 0.5 copy.34
  47.3 0.0 copy-done
  47.3 1.6 convolution_convert_fusion
  48.9 0.0 copy-start.2
  48.9 35.2 %all_to_all.15 = bf16[4,160,2048]{2,1,0:T(8,128)(2,1)S(1)} all-to-all(bf16[4,160,2048]{2,1,0:T(8,128)(2,1)S(1)} %bitcast.54), channel_id=1, replica_groups=mesh['sp'=64,'tp'=4] {'tp'}, dimensions={0} | all-to-all | bytes 5242880 | tf_op jit(solution)/shard_map/all_to_all | solution.py:46
  84.1 0.0 copy-start.4
  84.2 0.5 convert_reduce_fusion.1
  84.6 0.0 copy-done.2
  84.7 0.3 fusion.22
  84.9 0.0 copy-done.4
  85.0 0.2 fusion.24
  85.2 0.3 broadcast_in_dim.12
  85.5 35.0 %all_to_all.16 = bf16[4,160,2048]{2,1,0:T(8,128)(2,1)} all-to-all(bf16[4,160,2048]{2,1,0:T(8,128)(2,1)S(1)} %broadcast_in_dim.12), channel_id=1, replica_groups=mesh['sp'=64,'tp'=4] {'tp'}, dimensions={0} | all-to-all | bytes 5242880 | tf_op jit(solution)/shard_map/all_to_all | solution.py:52
  120.5 0.0 all-gather.2.cloned.1.call-done
  120.5 9.4 %fusion.6 = f32[640,1408]{1,0:T(8,128)} fusion(bf16[640,2048]{1,0:T(8,128)(2,1)} %bitcast.51, bf16[2048,4224]{1,0:T(8,128)(2,1)} %all-gather.2.cloned.1.call-done), kind=kOutput, calls=%fused_computation.9 | convolution fusion | flops 3690987520 | bytes 11993088 | tf_op jit(solution)/shard_map/dot_general | solution.py:149
  129.9 16.1 %fusion.15 = bf16[640,2048]{1,0:T(8,128)(2,1)} fusion(bf16[2048,4224]{1,0:T(8,128)(2,1)} %all-gather.2.cloned.1.call-done, bf16[640,2048]{1,0:T(8,128)(2,1)} %bitcast.52, f32[640,1408]{1,0:T(8,128)} %fusion.6), kind=kOutput, calls=%fused_computation.16 | convolution fusion | flops 7388692480 | bytes 20381696 | tf_op jit(solution)/shard_map/dot_general | solution.py:154
  146.0 34.4 %all_to_all.17 = bf16[4,160,2048]{2,1,0:T(8,128)(2,1)S(1)} all-to-all(bf16[4,160,2048]{2,1,0:T(8,128)(2,1)} %bitcast.53), channel_id=1, replica_groups=mesh['sp'=64,'tp'=4] {'tp'}, dimensions={0} | all-to-all | bytes 5242880 | tf_op jit(solution)/shard_map/all_to_all | solution.py:46
  180.4 0.5 convert_reduce_fusion
  180.9 1.0 fusion.25
  (7 shorter events, 0.1 us)
Async XLA Ops:
  6.5 40.8 %copy-start = (bf16[512,2048]{1,0:T(8,128)(2,1)S(1)}, bf16[512,2048]{1,0:T(8,128)(2,1)}, u32[]{:S(2)}) copy-start(bf16[512,2048]{1,0:T(8,128)(2,1)} %param.15) | copy-start | bytes 6291460
  6.5 113.9 %all-gather.2.cloned.1.call-start = ((), (), s32[]{:S(2)}) async-start(), calls=%async_computation.3 | async-start | bytes 17571840 | tf_op jit(solution)/shard_map/all_gather | solution.py:30
  11.1 5.2 %copy-start.1 = (bf16[640,2,64]{0,2,1:T(8,128)(2,1)}, bf16[640,2,64]{0,2,1:T(8,128)(2,1)S(1)}, u32[]{:S(2)}) copy-start(bf16[640,2,64]{0,2,1:T(8,128)(2,1)S(1)} %pad_maximum_fusion.8) | copy-start | bytes 491524
  11.8 14.1 %collective-permute-start = (bf16[128,256]{0,1:T(8,128)(2,1)}, bf16[128,256]{0,1:T(8,128)(2,1)}, u32[]{:S(2)}, u32[]{:S(2)}) collective-permute-start(bf16[128,256]{0,1:T(8,128)(2,1)} %get-tuple-element.16), channel_id=1, source_target_pairs={{0,4},{4,8},{8,12},{12,16},{16,20},{20,24},{24,28},{28,32},{32,36}... | collective-permute-start | bytes 196616 | tf_op jit(solution)/shard_map/ppermute | solution.py:18
  16.3 9.6 %collective-permute-start.1 = (bf16[128,256]{0,1:T(8,128)(2,1)}, bf16[128,256]{0,1:T(8,128)(2,1)}, u32[]{:S(2)}, u32[]{:S(2)}) collective-permute-start(bf16[128,256]{0,1:T(8,128)(2,1)} %get-tuple-element.17), channel_id=1, source_target_pairs={{4,0},{8,4},{12,8},{16,12},{20,16},{24,20},{28,24},{32,28},{36,32}... | collective-permute-start | bytes 196616 | tf_op jit(solution)/shard_map/ppermute | solution.py:20
  40.1 2.3 %copy-start.5 = (f32[2,4]{1,0:T(2,128)S(1)}, f32[2,4]{1,0:T(2,128)}, u32[]{:S(2)}) copy-start(f32[2,4]{1,0:T(2,128)} %max.17) | copy-start | bytes 100
  42.4 2.0 %copy-start.3 = (bf16[5,384,128]{1,2,0:T(8,128)(2,1)S(1)}, bf16[5,384,128]{1,2,0:T(8,128)(2,1)}, u32[]{:S(2)}) copy-start(bf16[5,384,128]{1,2,0:T(8,128)(2,1)} %copy.29) | copy-start | bytes 1474564
  48.9 35.8 %copy-start.2 = (bf16[160,2048]{1,0:T(8,128)(2,1)S(1)}, bf16[160,2048]{1,0:T(8,128)(2,1)}, u32[]{:S(2)}) copy-start(bf16[160,2048]{1,0:T(8,128)(2,1)} %param.14) | copy-start | bytes 1966084
  84.1 0.8 copy-start.4
Sparse Core Ops, SparseCore 0:
  10.1 104.6 all-gather.1
where the time goes:
time: 192 us; the launch traced here: 189 us
  blocking collectives  105 us (55%)
  matrix products  31.8 us (17%)
  local copies, waits for them, and re-layouts  18.3 us (10%)
  between operations  13.6 us (7%)
  other arithmetic  13.5 us (7%)
  starting transfers between devices  7 us (4%)
    all_to_all x2, blocking collectives, sent_and_summed(): lax.all_to_all(tiles, axis, split_axis=0, concat_axis=0, tiled=True)  69.7 us
    all_to_all x1, blocking collectives, copy_for_each(): return lax.all_to_all(copies, axis, split_axis=0, concat_axis=0, tiled=True)  35 us
    dot_general x1, matrix products, local(): jnp.dot(rows, down_whole, preferred_element_type=jnp.float32)  16.1 us
    dot_general x1, matrix products, local(): gate = jnp.dot(piece, gate_whole, preferred_element_type=jnp.float32)  9.4 us
    ppermute x1, starting transfers between devices, padded_2(): lax.ppermute(tail, axis, [(i, (i + 1) % count) for i in range(ends)])  4.49 us
  transfers between devices with their start and end apart: 3, of which 0 were waited for; matrix products, arithmetic and copies ran while one was open for 18% of the time, Pallas kernels for 0%

commit v1 on v0

v1 whole, which is shorter than its diff:
```python
import jax
import jax.numpy as jnp
import numpy as np
from jax import lax
from jax.experimental import pallas as pl
from jax.experimental.pallas import tpu as pltpu
from jax.sharding import PartitionSpec as P

HEAD = 64
WINDOW = 128
MESH = pl.DeviceIdType.MESH
BF = jnp.bfloat16
F32 = jnp.float32

NZ, NX, NC, NY = 8, 4, 2, 4
ROWS = 32
TOK = 640
BLK = TOK // NY
HALF = BLK // 2
EXT = TOK + 2 * WINDOW
PAD = 3 * BLK + 4 * WINDOW
D = 2048
FFL = 1408
GB = 1280
CB = 2 * GB
CA = 2 * (FFL - GB) + FFL
QW = 512
NSEM = 112


def tables():
    lane = (np.arange(128) % 64) % 32
    freq = 1.0 / 10000.0 ** (2.0 * lane / HEAD)
    near = (np.arange(EXT) - WINDOW)[:, None] * freq[None]
    far = (np.arange(NZ * NX * NC) * TOK)[:, None] * freq[None]
    return np.concatenate([np.cos(near), np.sin(near), np.cos(far), np.sin(far)], 0).astype(np.float32)


def nt(a, b):
    return lax.dot_general(a, b, (((1,), (1,)), ((), ())), preferred_element_type=F32)


def mm(a, b):
    return jnp.dot(a, b, preferred_element_type=F32)


def kernel(
    q_hbm, k_hbm, v_hbm, sink, st_hbm, ow_hbm, gain, g_hbm, u_hbm, d_hbm, tab_hbm,
    out,
    wa, wb, tab, q, qr, kv, kk, vv, ow, dn, st, bias, att,
    pb1, s1, f1, pb2, s2, f2, mixed, xs, hid,
    lsem, ssem, rsem,
):
    s = lax.axis_index("sp")
    y = lax.axis_index("tp")
    c = s % NC
    x = (s // NC) % NX
    z = s // (NC * NX)

    def at(zz, xx, cc):
        return ((zz % NZ) * NX + xx % NX) * NC + cc

    ydev = {1: (s, (y + 1) % NY), -1: (s, (y + NY - 1) % NY)}
    xdev = {1: (at(z, x + 1, c), y), -1: (at(z, x + NX - 1, c), y)}
    zdev = {1: (at(z + 1, x, c), y), -1: (at(z + NZ - 1, x, c), y)}
    mate = (at(z, x, 1 - c), y)
    nsp = NZ * NX * NC
    hdev = {1: ((s + 1) % nsp, y), -1: ((s + nsp - 1) % nsp, y)}

    loads = {}

    def load(name, src, dst):
        cp = pltpu.make_async_copy(src, dst, lsem.at[len(loads)])
        cp.start()
        loads[name] = cp

    rest = FFL - GB
    load("gb", g_hbm.at[:, pl.ds(0, GB)], wb.at[z, x, c, :, pl.ds(0, GB)])
    load("ub", u_hbm.at[:, pl.ds(0, GB)], wb.at[z, x, c, :, pl.ds(GB, GB)])
    load("d", d_hbm, dn)
    load("ga", g_hbm.at[:, pl.ds(GB, rest)], wa.at[z, x, c, :, pl.ds(0, rest)])
    load("ua", u_hbm.at[:, pl.ds(GB, rest)], wa.at[z, x, c, :, pl.ds(rest, rest)])
    load("k", k_hbm, kv.at[0, pl.ds(WINDOW, TOK)])
    load("v", v_hbm, kv.at[1, pl.ds(WINDOW, TOK)])
    load("tab", tab_hbm, tab)
    load("q", q_hbm, q)
    load("ow", ow_hbm, ow)
    load("st", st_hbm, st)

    barrier = pltpu.get_barrier_semaphore()
    for dev in (*ydev.values(), *xdev.values(), *zdev.values(), mate, *hdev.values()):
        pl.semaphore_signal(barrier, inc=1, device_id=dev, device_id_type=MESH)
    pl.semaphore_wait(barrier, 9)

    slots = {}
    sent = []

    def copy(name, src, dst, dev):
        i = slots.setdefault(name, len(slots))
        return pltpu.make_async_remote_copy(
            src_ref=src, dst_ref=dst, send_sem=ssem.at[i], recv_sem=rsem.at[i], device_id=dev, device_id_type=MESH
        )

    def send(name, ref, dev, dst=None):
        cp = copy(name, ref, ref if dst is None else dst, dev)
        cp.start()
        sent.append(cp)

    def recv(name, ref):
        copy(name, ref, ref, mate).wait_recv()

    def zb(dz, half=None):
        ref = wb.at[(z + dz + NZ) % NZ, x, c]
        return ref if half is None else ref.at[pl.ds(16 * half, 16)]

    def xb(dz, dx, half=None):
        ref = wb.at[(z + dz + NZ) % NZ, (x + dx + NX) % NX, c]
        return ref if half is None else ref.at[pl.ds(16 * half, 16)]

    def za(dz, half=None):
        zz = (z + dz + NZ) % NZ
        return wa.at[zz, :, c] if half is None else wa.at[zz, pl.ds(2 * half, 2), c]

    def xa(dx, half=None):
        ref = wa.at[z, (x + dx + NX) % NX, c]
        return ref if half is None else ref.at[pl.ds(16 * half, 16)]

    def bx_send(dz):
        for r in (1, -1):
            send(("bx", dz, r), xb(dz, 0), xdev[r])

    def bx_mid(dz):
        for r, half in ((1, 0), (-1, 1)):
            recv(("bx", dz, r), xb(dz, -r))
            send(("bh", dz, r), xb(dz, -r, half), xdev[r])

    def bx_end(dz):
        for r, half in ((1, 0), (-1, 1)):
            recv(("bh", dz, r), xb(dz, -2 * r, half))
        zz = (z + dz + NZ) % NZ
        send(("bm", dz), wb.at[zz, :, c], mate)

    def bz(n):
        for r, half in ((1, 0), (-1, 1)):
            if n < 4:
                recv(("bz", r, n), zb(-r * n))
                if n < 3:
                    send(("bz", r, n + 1), zb(-r * n), zdev[r])
                else:
                    send(("bz", r, 4), zb(-r * 3, half), zdev[r])
            else:
                recv(("bz", r, 4), zb(-r * 4, half))
        if n < 4:
            bx_send(n)
            bx_send(-n)
        else:
            bx_send(4)

    def az(n):
        for r, half in ((1, 0), (-1, 1)):
            if n < 4:
                recv(("az", r, n), za(-r * n))
                if n < 3:
                    send(("az", r, n + 1), za(-r * n), zdev[r])
                else:
                    send(("az", r, 4), za(-r * 3, half), zdev[r])
            else:
                recv(("az", r, 4), za(-r * 4, half))
        for dz in (n, -n) if n < 4 else (4,):
            send(("am", dz), za(dz), mate)

    def ax_mid():
        for r, half in ((1, 0), (-1, 1)):
            recv(("ax", r), xa(-r))
            send(("ah", r), xa(-r, half), xdev[r])

    def ax_end():
        for r, half in ((1, 0), (-1, 1)):
            recv(("ah", r), xa(-2 * r, half))
        for r in (1, -1):
            send(("az", r, 1), za(0), zdev[r])
        send(("am", 0), za(0), mate)

    def mates():
        for dz in (0, 1, -1, 2, -2, 3, -3, 4):
            zz = (z + dz + NZ) % NZ
            recv(("bm", dz), wb.at[zz, :, 1 - c])
            recv(("am", dz), wa.at[zz, :, 1 - c])

    loads["gb"].wait()
    loads["ub"].wait()
    for r in (1, -1):
        send(("bz", r, 1), zb(0), zdev[r])
    loads["k"].wait()
    loads["v"].wait()
    send(("halo", -1), kv.at[:, pl.ds(WINDOW, WINDOW)], hdev[-1], kv.at[:, pl.ds(WINDOW + TOK, WINDOW)])
    send(("halo", 1), kv.at[:, pl.ds(TOK, WINDOW)], hdev[1], kv.at[:, pl.ds(0, WINDOW)])
    loads["d"].wait()
    eye = (
        lax.broadcasted_iota(jnp.int32, (ROWS, ROWS), 0) == lax.broadcasted_iota(jnp.int32, (ROWS, ROWS), 1)
    ).astype(F32).astype(BF)
    wa[z, x, c, :, 2 * rest :] = nt(eye, dn[...]).astype(BF)
    loads["ga"].wait()
    loads["ua"].wait()
    for r in (1, -1):
        send(("ax", r), xa(0), xdev[r])
    bx_send(0)

    loads["tab"].wait()
    cb = tab[pl.ds(2 * EXT + s, 1), :]
    sb = tab[pl.ds(2 * EXT + nsp + s, 1), :]

    def rotate(rows, value):
        cl, sl = tab[rows, :], tab[pl.ds(EXT + rows.start, rows.size), :]
        cos = cb * cl - sb * sl
        sin = sb * cl + cb * sl
        return value.astype(F32) * cos + mm(value, turn) * sin

    jj = lax.broadcasted_iota(jnp.int32, (128, 128), 0)
    ii = lax.broadcasted_iota(jnp.int32, (128, 128), 1)
    low = (ii % 64) < 32
    turn = (jnp.where(jj == ii - 32, jnp.where(low, 0.0, 1.0), 0.0)
            - jnp.where(jj == ii + 32, jnp.where(low, 1.0, 0.0), 0.0)).astype(BF)
    flip = jnp.where((jj + 64) % 128 == ii, 1.0, 0.0).astype(BF)

    loads["q"].wait()
    for t in range(4):
        qr[t] = rotate(pl.ds(WINDOW, TOK), q[:, 128 * t : 128 * (t + 1)]).astype(BF)
    ax_mid()
    recv(("halo", -1), kv.at[:, pl.ds(WINDOW + TOK, WINDOW)])
    recv(("halo", 1), kv.at[:, pl.ds(0, WINDOW)])
    lane = lax.broadcasted_iota(jnp.int32, (EXT, 128), 1)
    left = lane < 64
    zero = jnp.zeros((EXT, 128), BF)
    one = jnp.where(left, 1.0, 0.0).astype(BF)
    two = jnp.where(left, 0.0, 1.0).astype(BF)
    kr = rotate(pl.ds(0, EXT), kv[0]).astype(BF)
    ks = mm(kr, flip)
    kr = kr.astype(F32)
    vr = kv[1].astype(F32)
    vs = mm(kv[1], flip)
    for i in range(4):
        kk[i, EXT:, :] = jnp.zeros((PAD - EXT, 128), BF)
        vv[i, EXT:, :] = jnp.zeros((PAD - EXT, 256), BF)
        ksrc, vsrc = ((kr, vr), (ks, vs), (ks, vs), (kr, vr))[i]
        keep = left if i % 2 == 0 else lane >= 64
        kk[i, :EXT, :] = jnp.where(keep, ksrc, 0.0).astype(BF)
        vv[i, :EXT, :128] = jnp.where(keep, vsrc, 0.0).astype(BF)
        vv[i, :EXT, 128:] = one if i % 2 == 0 else two

    def attend(b):
        first = s * TOK + b * BLK
        ri = lax.broadcasted_iota(jnp.int32, (BLK, QW), 0)
        ci = lax.broadcasted_iota(jnp.int32, (BLK, QW), 1)
        lo = jnp.maximum(ri, WINDOW - first)
        hi = jnp.minimum(ri + 2 * WINDOW, nsp * TOK - 1 + WINDOW - first)
        bias[...] = jnp.where((ci >= lo) & (ci <= hi), 0.0, -jnp.inf)
        rows = pl.multiple_of(b * BLK, 32)
        half = lax.broadcasted_iota(jnp.int32, (BLK, 128), 1) < 64

        def tile(t, carry):
            qt = qr[t, pl.ds(rows, BLK), :]
            acc, ends = None, []
            for par in range(2):
                i = (t // 2) * 2 + par
                sc = nt(qt, kk[i, pl.ds(rows, QW), :]) * 0.125 + bias[...]
                snk = sink[2 * t + par]
                top = jnp.maximum(jnp.max(sc, axis=1, keepdims=True), snk)
                prob = jnp.exp(sc - top).astype(BF)
                part = mm(prob, vv[i, pl.ds(rows, QW), :])
                acc = part if acc is None else acc + part
                ends.append(jnp.exp(snk - top))
            den = acc[:, 128:] + jnp.where(half, ends[0], ends[1])
            att[:, pl.ds(pl.multiple_of(t * 128, 128), 128)] = (acc[:, :128] / den).astype(BF)
            return carry

        lax.fori_loop(0, 4, tile, 0)

    def project(slot):
        def cols(n, carry):
            at_n = pl.ds(pl.multiple_of(n * 512, 512), 512)
            pb1[slot, :, at_n] = mm(att[...], ow[:, at_n]).astype(BF)
            return carry

        lax.fori_loop(0, 4, cols, 0)

    UP, LOW = pl.ds(0, HALF), pl.ds(HALF, HALF)
    part_of = {1: (0, UP, LOW), -1: (1, LOW, UP)}

    def rs_far(tag, pb, sbuf):
        for r in (1, -1):
            j, rel, _ = part_of[r]
            send((tag, "s", r), pb.at[0, rel], ydev[r], sbuf.at[j])

    def rs_near(tag, pb, fbuf, r):
        j, _, direct = part_of[r]
        send((tag, "d", r), pb.at[1 + j, direct], ydev[r], fbuf.at[j, direct])

    def rs_relay(tag, pb, sbuf, fbuf):
        for r in (1, -1):
            j, rel, _ = part_of[r]
            recv((tag, "s", r), sbuf.at[j])
            pb[1 + j, rel, :] = (pb[1 + j, rel, :].astype(F32) + sbuf[j].astype(F32)).astype(BF)
            send((tag, "r", r), pb.at[1 + j, rel], ydev[r], fbuf.at[j, rel])

    def rs_sum(tag, pb, fbuf):
        for r in (1, -1):
            j, rel, direct = part_of[r]
            recv((tag, "d", r), fbuf.at[j, direct])
            recv((tag, "r", r), fbuf.at[j, rel])
        return pb[3].astype(F32) + fbuf[0].astype(F32) + fbuf[1].astype(F32)

    ynext = {2: (y + 2) % NY, 1: (y + 1) % NY, -1: (y + NY - 1) % NY, 0: y}

    bx_mid(0)
    attend(ynext[2])
    loads["ow"].wait()
    project(0)
    rs_far("r1", pb1, s1)
    bz(1)
    ax_end()
    attend(ynext[1])
    project(1)
    rs_near("r1", pb1, f1, 1)
    bx_end(0)
    attend(ynext[-1])
    project(2)
    rs_near("r1", pb1, f1, -1)
    bz(2)
    attend(y)
    project(3)
    bx_mid(1)
    bx_mid(-1)
    rs_relay("r1", pb1, s1, f1)
    az(1)
    bz(3)
    bx_end(1)
    bx_end(-1)
    bx_mid(2)
    bx_mid(-2)
    loads["st"].wait()
    total = st[...].astype(F32) + rs_sum("r1", pb1, f1)
    mixed[...] = total.astype(BF)
    wide = mixed[...].astype(F32)
    scale = lax.rsqrt(jnp.mean(wide * wide, axis=1, keepdims=True) + 1e-06)
    xs[y] = (wide * scale * gain[...]).astype(BF)
    for r in (1, -1):
        for part in part_of[r][1:]:
            send(("g", r, part is UP), xs.at[y, part], ydev[r])
    az(2)
    bz(4)
    bx_end(2)
    bx_end(-2)
    for r in (1, -1):
        rel = part_of[r][1]
        recv(("g", r, rel is UP), xs.at[ynext[-r], rel])
        send(("gh", r), xs.at[ynext[-r], rel], ydev[r])
    bx_mid(3)
    bx_mid(-3)
    az(3)
    bx_end(3)
    bx_end(-3)
    bx_mid(4)
    for r in (1, -1):
        direct = part_of[r][2]
        recv(("g", r, direct is UP), xs.at[ynext[-r], direct])
    az(4)
    bx_end(4)
    mates()

    def feed(b, slot):
        def cols(n, carry):
            gu = []
            for base in (0, GB):
                w = wb[:, :, :, :, pl.ds(pl.multiple_of(base + n * 256, 256), 256)].reshape(D, 256)
                gu.append(mm(xs[b], w))
            hid[:, pl.ds(pl.multiple_of(n * 256, 256), 256)] = (gu[0] / (1.0 + jnp.exp(-gu[0])) * gu[1]).astype(BF)
            return carry

        lax.fori_loop(0, GB // 256, cols, 0)
        gu = mm(xs[b], wa[:, :, :, :, : 2 * rest].reshape(D, 2 * rest))
        gate, upward = gu[:, :rest], gu[:, rest:]
        hid[:, GB:] = (gate / (1.0 + jnp.exp(-gate)) * upward).astype(BF)

        def down(n, carry):
            w = wa[n, :, :, :, 2 * rest :].reshape(256, FFL)
            pb2[slot, :, pl.ds(pl.multiple_of(n * 256, 256), 256)] = nt(hid[...], w).astype(BF)
            return carry

        lax.fori_loop(0, D // 256, down, 0)

    feed(ynext[1], 1)
    rs_near("r2", pb2, f2, 1)
    feed(ynext[-1], 2)
    rs_near("r2", pb2, f2, -1)
    for r in (1, -1):
        rel = part_of[r][1]
        recv(("gh", r), xs.at[ynext[2], rel])
    feed(ynext[2], 0)
    rs_far("r2", pb2, s2)
    feed(y, 3)
    rs_relay("r2", pb2, s2, f2)
    out[...] = (mixed[...].astype(F32) + 0.5 * rs_sum("r2", pb2, f2)).astype(BF)
    for cp in sent:
        cp.wait_send()
    assert len(slots) <= NSEM


def local(queries, keys, values, sink, stream, out_weight, norm_gain, gate_weight, up_weight, down_weight):
    hbm = pl.BlockSpec(memory_space=pl.ANY)
    vmem = pl.BlockSpec(memory_space=pltpu.VMEM)
    smem = pl.BlockSpec(memory_space=pltpu.SMEM)
    V = pltpu.VMEM
    return pl.pallas_call(
        kernel,
        name="layer",
        out_shape=jax.ShapeDtypeStruct((BLK, D), BF),
        in_specs=[hbm, hbm, hbm, smem, hbm, hbm, vmem, hbm, hbm, hbm, hbm],
        out_specs=vmem,
        scratch_shapes=[
            V((NZ, NX, NC, ROWS, CA), BF),
            V((NZ, NX, NC, ROWS, CB), BF),
            V((2 * EXT + 2 * NZ * NX * NC, 128), F32),
            V((TOK, 512), BF),
            V((4, TOK, 128), BF),
            V((2, EXT, 128), BF),
            V((4, PAD, 128), BF),
            V((4, PAD, 256), BF),
            V((512, D), BF),
            V((FFL, ROWS), BF),
            V((BLK, D), BF),
            V((BLK, QW), F32),
            V((BLK, 512), BF),
            V((4, BLK, D), BF),
            V((2, HALF, D), BF),
            V((2, BLK, D), BF),
            V((4, BLK, D), BF),
            V((2, HALF, D), BF),
            V((2, BLK, D), BF),
            V((BLK, D), BF),
            V((NY, BLK, D), BF),
            V((BLK, FFL), BF),
            pltpu.SemaphoreType.DMA((11,)),
            pltpu.SemaphoreType.DMA((NSEM,)),
            pltpu.SemaphoreType.DMA((NSEM,)),
        ],
        compiler_params=pltpu.CompilerParams(
            collective_id=0, has_side_effects=True, vmem_limit_bytes=62 * 1024 * 1024
        ),
    )(
        queries, keys, values, sink, stream, out_weight, norm_gain.reshape(1, D),
        gate_weight, up_weight, down_weight, jnp.asarray(tables()),
    )


def solution(mesh):
    placed = (
        P("sp", "tp"), P("sp", "tp"), P("sp", "tp"), P("tp"), P(("sp", "tp"), None), P("tp", None), P(),
        P("sp", "tp"), P("sp", "tp"), P("tp", "sp"),
    )
    return jax.shard_map(local, mesh=mesh, in_specs=placed, out_specs=P(("sp", "tp"), None), check_vma=False)
```

time: 192 us -> 110 us (0.57); the launches traced: 189 us -> 110 us
  Pallas kernels: 0 us -> 106 us
  blocking collectives: 105 us -> 0 us
  matrix products: 31.8 us -> 0 us
  local copies, waits for them, and re-layouts: 18.3 us -> 3.78 us
  between operations: 13.6 us -> 0.01 us
  other arithmetic: 13.5 us -> 0 us
  starting transfers between devices: 7 us -> 0 us
    pallas_call x0 -> x1, Pallas kernels: none -> 106 us  [local(): pl.pallas_call(kernel, name='layer', out_shape=jax.ShapeDtypeStruct((BLK,...]
    all_to_all x3 -> x0, blocking collectives: 105 us -> none  [the longest x2 69.7 us: sent_and_summed(): lax.all_to_all(tiles, axis, split_axis=0, concat_axis=0, tiled=True)]
    dot_general x5 -> x0, matrix products: 31.8 us -> none  [the longest x1 16.1 us: local(): jnp.dot(rows, down_whole, preferred_element_type=jnp.float32)]
    slice x5 -> x0, local copies, waits for them, and re-layouts: 8.94 us -> none  [the longest x2 3.73 us: window_attend(): banded = jnp.concatenate([framed[:-2], framed[1:-1], framed[2:]], axis=1)]
    ppermute x2 -> x0, starting transfers between devices: 7 us -> none  [the longest x1 4.49 us: padded_2(): lax.ppermute(tail, axis, [(i, (i + 1) % count) for i in range(ends)])]
    concatenate x6 -> x0, other arithmetic: 6.81 us -> none  [the longest x1 2.12 us: padded_2(): jnp.concatenate([lax.ppermute(tail, axis, [(i, (i + 1) % count) for i in...]
    reduce_sum x4 -> x0, other arithmetic: 3.17 us -> none  [the longest x1 1.92 us: window_attend(): denom = jnp.sum(raised, -1) + jnp.exp(sink_grid - top)]
    convert_element_type x2 -> x0, local copies, waits for them, and re-layouts: 2.28 us -> none  [the longest x1 1.79 us: rotary(): return turned.reshape(length, -1).astype(jnp.bfloat16)]
  transfers between devices with their start and end apart: 3 -> 0, of which waited for: 0 -> 0; matrix products, arithmetic and copies ran while one was open for 18% -> 0% of each run, Pallas kernels for 0% -> 0%
where the time goes in v1:
time: 110 us
  Pallas kernels  106 us (96%)
  local copies, waits for them, and re-layouts  3.78 us (3%)
    pallas_call x1, Pallas kernels, local(): pl.pallas_call(kernel, name='layer', out_shape=jax.ShapeDtypeStruct((BLK,...  106 us
    unnamed x2, local copies, waits for them, and re-layouts  3.78 us

profile of v1, /device:TPU:1, one launch (start us, length us, event | category | flops | bytes accessed | tf_op | source)
XLA Modules:
  0.0 109.7 jit_solution(11920016256637366870)
XLA Ops:
  0.0 1.8 %copy.12.d_hbm = bf16[1408,32]{1,0:T(8,128)(2,1)} copy(bf16[1408,32]{0,1:T(8,128)(2,1)} %param.20) | data formatting | bytes 180224 | tf_op args[9]
  1.8 105.9 %layer.1 = bf16[160,2048]{1,0:T(8,128)(2,1)} custom-call(bf16[640,512]{1,0:T(8,128)(2,1)} %q_hbm.1, bf16[640,128]{1,0:T(8,128)(2,1)} %k_hbm.1, bf16[640,128]{1,0:T(8,128)(2,1)} %v_hbm.1, f32[8]{0:T(128)} %sink.1, bf16[160,2048]{1,0:T(8,128)(2,1)} %st_hbm.1, bf16[512,2048]{1,0:T(8,128)(2,1)} %ow_hbm.1, f32[1,2048]{1,0:T(1,128)} %bitcast.1, ...), custom_call_target="tpu_custom_call" | custom-call | tf_op jit(solution)/shard_map/layer/pallas_call | solution.py:414
  107.7 2.0 %copy.14 = bf16[160,2048]{1,0:T(8,128)(2,1)} copy(bf16[160,2048]{1,0:T(8,128)(2,1)} %layer.1) | data formatting | bytes 1310720

commit v2 on v1

v2 whole, which is shorter than its diff:
```python
import jax
import jax.numpy as jnp
import numpy as np
from jax import lax
from jax.experimental import pallas as pl
from jax.experimental.pallas import tpu as pltpu
from jax.sharding import PartitionSpec as P

HEAD = 64
WINDOW = 128
MESH = pl.DeviceIdType.MESH
BF = jnp.bfloat16
F32 = jnp.float32

NZ, NX, NC, NY = 8, 4, 2, 4
ROWS = 32
TOK = 640
BLK = TOK // NY
HALF = BLK // 2
EXT = TOK + 2 * WINDOW
PAD = 3 * BLK + 4 * WINDOW
D = 2048
FFL = 1408
GB = 1280
CB = 2 * GB
CA = 2 * (FFL - GB) + FFL
QW = 512
NSEM = 192
ORDER = (
    "begin", "turn_q", "prepare", "att_f", "bz_1", "proj_f", "ax_mid", "att_n", "proj_n", "az_1_0", "bm_0", "att_p",
    "rl+0", "bz_2", "proj_p", "rl-0", "bm_1", "att_o", "rl+1", "near+", "rl-1", "proj_o", "ax_end", "az_1_-1",
    "az_2_0", "be_0", "az_1_1", "bm_-1", "bm_2", "bz_3", "norm_U", "az_1_2", "bm_-2", "az_2_-1", "be_1", "be_-1",
    "az_3_0", "be_2", "norm_L", "az_2_1", "bz_4", "bm_3", "az_2_2", "bm_-3", "az_3_-1", "gU", "az_4_0", "be_-2",
    "az_3_1", "gL0", "bm_4", "az_3_2", "az_4_-1", "be_3", "gL1", "az_4_1", "be_-3", "az_4_2", "be_4", "feed1",
    "feed2", "feed3", "r2l0", "r2l1", "fin0", "fin1",
)
SUB = 2


def tables():
    lane = (np.arange(128) % 64) % 32
    freq = 1.0 / 10000.0 ** (2.0 * lane / HEAD)
    near = (np.arange(EXT) - WINDOW)[:, None] * freq[None]
    far = (np.arange(NZ * NX * NC) * TOK)[:, None] * freq[None]
    return np.concatenate([np.cos(near), np.sin(near), np.cos(far), np.sin(far)], 0).astype(np.float32)


def nt(a, b):
    return lax.dot_general(a, b, (((1,), (1,)), ((), ())), preferred_element_type=F32)


def mm(a, b):
    return jnp.dot(a, b, preferred_element_type=F32)


def kernel(
    q_hbm, k_hbm, v_hbm, sink, st_hbm, ow_hbm, gain, g_hbm, u_hbm, d_hbm, tab_hbm,
    out,
    wa, wb, tab, q, qr, kv, kk, vv, ow, st, bias, att,
    pb1, s1, f1, pb2, s2, f2, mixed, xs, hid,
    lsem, ssem, rsem,
):
    s = lax.axis_index("sp")
    y = lax.axis_index("tp")
    c = s % NC
    x = (s // NC) % NX
    z = s // (NC * NX)

    def at(zz, xx, cc):
        return ((zz % NZ) * NX + xx % NX) * NC + cc

    ydev = {1: (s, (y + 1) % NY), -1: (s, (y + NY - 1) % NY)}
    xdev = {1: (at(z, x + 1, c), y), -1: (at(z, x + NX - 1, c), y)}
    zdev = {1: (at(z + 1, x, c), y), -1: (at(z + NZ - 1, x, c), y)}
    mate = (at(z, x, 1 - c), y)
    nsp = NZ * NX * NC
    hdev = {1: ((s + 1) % nsp, y), -1: ((s + nsp - 1) % nsp, y)}

    barrier = pltpu.get_barrier_semaphore()
    for dev in (*ydev.values(), *xdev.values(), *zdev.values(), mate, *hdev.values()):
        pl.semaphore_signal(barrier, inc=1, device_id=dev, device_id_type=MESH)

    loads = {}

    def load(name, src, dst):
        cp = pltpu.make_async_copy(src, dst, lsem.at[len(loads)])
        cp.start()
        loads[name] = cp

    rest = FFL - GB
    load("k", k_hbm, kv.at[0, pl.ds(WINDOW, TOK)])
    load("v", v_hbm, kv.at[1, pl.ds(WINDOW, TOK)])
    load("gb", g_hbm.at[:, pl.ds(0, GB)], wb.at[z, x, c, :, pl.ds(0, GB)])
    load("ub", u_hbm.at[:, pl.ds(0, GB)], wb.at[z, x, c, :, pl.ds(GB, GB)])
    load("da", d_hbm, wa.at[z, x, c, :, pl.ds(2 * rest, FFL)])
    load("ga", g_hbm.at[:, pl.ds(GB, rest)], wa.at[z, x, c, :, pl.ds(0, rest)])
    load("ua", u_hbm.at[:, pl.ds(GB, rest)], wa.at[z, x, c, :, pl.ds(rest, rest)])
    load("tab", tab_hbm, tab)
    load("q", q_hbm, q)
    load("ow", ow_hbm, ow)
    load("st", st_hbm, st)

    def greet():
        pl.semaphore_wait(barrier, 9)

    greet()

    slots = {}
    sent = []

    def copy(name, src, dst, dev):
        i = slots.setdefault(name, len(slots))
        return pltpu.make_async_remote_copy(
            src_ref=src, dst_ref=dst, send_sem=ssem.at[i], recv_sem=rsem.at[i], device_id=dev, device_id_type=MESH
        )

    def send(name, ref, dev, dst=None):
        cp = copy(name, ref, ref if dst is None else dst, dev)
        cp.start()
        sent.append(cp)

    def recv(name, ref):
        copy(name, ref, ref, mate).wait_recv()

    def zb(dz, half=None):
        ref = wb.at[(z + dz + NZ) % NZ, x, c]
        return ref if half is None else ref.at[pl.ds(16 * half, 16)]

    def xb(dz, dx, half=None):
        ref = wb.at[(z + dz + NZ) % NZ, (x + dx + NX) % NX, c]
        return ref if half is None else ref.at[pl.ds(16 * half, 16)]

    def za(dz, dx, half=None):
        ref = wa.at[(z + dz + NZ) % NZ, (x + dx + NX) % NX, c]
        return ref if half is None else ref.at[pl.ds(16 * half, 16)]

    def xa(dx, half=None):
        ref = wa.at[z, (x + dx + NX) % NX, c]
        return ref if half is None else ref.at[pl.ds(16 * half, 16)]

    def bx_send(dz):
        for r in (1, -1):
            send(("bx", dz, r), xb(dz, 0), xdev[r])

    def bx_mid(dz):
        for r, half in ((1, 0), (-1, 1)):
            recv(("bx", dz, r), xb(dz, -r))
            send(("bh", dz, r), xb(dz, -r, half), xdev[r])

    def bx_end(dz):
        for r, half in ((1, 0), (-1, 1)):
            recv(("bh", dz, r), xb(dz, -2 * r, half))
        zz = (z + dz + NZ) % NZ
        send(("bm", dz), wb.at[zz, :, c], mate)

    def bz(n):
        for r, half in ((1, 0), (-1, 1)):
            if n < 4:
                recv(("bz", r, n), zb(-r * n))
                if n < 3:
                    send(("bz", r, n + 1), zb(-r * n), zdev[r])
                else:
                    send(("bz", r, 4), zb(-r * 3, half), zdev[r])
            else:
                recv(("bz", r, 4), zb(-r * 4, half))
        if n < 4:
            bx_send(n)
            bx_send(-n)
        else:
            bx_send(4)

    def az_send(n, dx, r):
        if n < 4:
            send(("az", r, n, dx), za(-r * (n - 1), dx), zdev[r])
        else:
            half = 0 if r == 1 else 1
            send(("az", r, 4, dx), za(-r * 3, dx, half), zdev[r])

    parts = {}

    def az(n, *dxs):
        for dx in dxs:
            for r, half in ((1, 0), (-1, 1)):
                if n < 4:
                    recv(("az", r, n, dx), za(-r * n, dx))
                    az_send(n + 1, dx, r)
                else:
                    recv(("az", r, 4, dx), za(-r * 4, dx, half))
            parts[n] = parts.get(n, 0) + 1
            if parts[n] == NX:
                for dz in (n, -n) if n < 4 else (4,):
                    send(("am", dz), wa.at[(z + dz + NZ) % NZ, :, c], mate)

    def ax_mid():
        for r, half in ((1, 0), (-1, 1)):
            recv(("ax", r), xa(-r))
            send(("ah", r), xa(-r, half), xdev[r])
        for r in (1, -1):
            for dx in (1, -1):
                az_send(1, dx, r)

    def ax_end():
        for r, half in ((1, 0), (-1, 1)):
            recv(("ah", r), xa(-2 * r, half))
        for r in (1, -1):
            az_send(1, 2, r)
        send(("am", 0), wa.at[z, :, c], mate)

    def mates():
        for dz in (0, 1, -1, 2, -2, 3, -3, 4):
            zz = (z + dz + NZ) % NZ
            recv(("bm", dz), wb.at[zz, :, 1 - c])
            recv(("am", dz), wa.at[zz, :, 1 - c])

    def begin():
        loads["k"].wait()
        loads["v"].wait()
        send(("halo", -1), kv.at[:, pl.ds(WINDOW, WINDOW)], hdev[-1], kv.at[:, pl.ds(WINDOW + TOK, WINDOW)])
        send(("halo", 1), kv.at[:, pl.ds(TOK, WINDOW)], hdev[1], kv.at[:, pl.ds(0, WINDOW)])
        for name in ("gb", "ub", "ga", "ua", "da"):
            loads[name].wait()
        for r in (1, -1):
            send(("bz", r, 1), zb(0), zdev[r])
            send(("ax", r), xa(0), xdev[r])
        for r in (1, -1):
            az_send(1, 0, r)
        bx_send(0)

    loads["tab"].wait()
    cb = tab[pl.ds(2 * EXT + s, 1), :]
    sb = tab[pl.ds(2 * EXT + nsp + s, 1), :]

    def rotate(rows, value):
        cl, sl = tab[rows, :], tab[pl.ds(EXT + rows.start, rows.size), :]
        cos = cb * cl - sb * sl
        sin = sb * cl + cb * sl
        return value.astype(F32) * cos + mm(value, turn) * sin

    jj = lax.broadcasted_iota(jnp.int32, (128, 128), 0)
    ii = lax.broadcasted_iota(jnp.int32, (128, 128), 1)
    low = (ii % 64) < 32
    turn = (jnp.where(jj == ii - 32, jnp.where(low, 0.0, 1.0), 0.0)
            - jnp.where(jj == ii + 32, jnp.where(low, 1.0, 0.0), 0.0)).astype(BF)
    flip = jnp.where((jj + 64) % 128 == ii, 1.0, 0.0).astype(BF)

    def turn_q():
        loads["q"].wait()
        for t in range(4):
            qr[t] = rotate(pl.ds(WINDOW, TOK), q[:, 128 * t : 128 * (t + 1)]).astype(BF)

    def prepare():
        recv(("halo", -1), kv.at[:, pl.ds(WINDOW + TOK, WINDOW)])
        recv(("halo", 1), kv.at[:, pl.ds(0, WINDOW)])
        lane = lax.broadcasted_iota(jnp.int32, (EXT, 128), 1)
        left = lane < 64
        one = jnp.where(left, 1.0, 0.0).astype(BF)
        two = jnp.where(left, 0.0, 1.0).astype(BF)
        kr = rotate(pl.ds(0, EXT), kv[0]).astype(BF)
        ks = mm(kr, flip)
        kr = kr.astype(F32)
        vr = kv[1].astype(F32)
        vs = mm(kv[1], flip)
        for i in range(4):
            kk[i, EXT:, :] = jnp.zeros((PAD - EXT, 128), BF)
            vv[i, EXT:, :] = jnp.zeros((PAD - EXT, 256), BF)
            ksrc, vsrc = ((kr, vr), (ks, vs), (ks, vs), (kr, vr))[i]
            keep = left if i % 2 == 0 else lane >= 64
            kk[i, :EXT, :] = jnp.where(keep, ksrc, 0.0).astype(BF)
            vv[i, :EXT, :128] = jnp.where(keep, vsrc, 0.0).astype(BF)
            vv[i, :EXT, 128:] = one if i % 2 == 0 else two

    def attend(b):
        first = s * TOK + b * BLK
        ri = lax.broadcasted_iota(jnp.int32, (BLK, QW), 0)
        ci = lax.broadcasted_iota(jnp.int32, (BLK, QW), 1)
        lo = jnp.maximum(ri, WINDOW - first)
        hi = jnp.minimum(ri + 2 * WINDOW, nsp * TOK - 1 + WINDOW - first)
        bias[...] = jnp.where((ci >= lo) & (ci <= hi), 0.0, -jnp.inf)
        rows = pl.multiple_of(b * BLK, 32)
        half = lax.broadcasted_iota(jnp.int32, (BLK, 128), 1) < 64

        def tile(t, carry):
            qt = qr[t, pl.ds(rows, BLK), :]
            acc, ends = None, []
            for par in range(2):
                i = (t // 2) * 2 + par
                sc = nt(qt, kk[i, pl.ds(rows, QW), :]) * 0.125 + bias[...]
                snk = sink[2 * t + par]
                top = jnp.maximum(jnp.max(sc, axis=1, keepdims=True), snk)
                prob = jnp.exp(sc - top).astype(BF)
                part = mm(prob, vv[i, pl.ds(rows, QW), :])
                acc = part if acc is None else acc + part
                ends.append(jnp.exp(snk - top))
            den = acc[:, 128:] + jnp.where(half, ends[0], ends[1])
            att[:, pl.ds(pl.multiple_of(t * 128, 128), 128)] = (acc[:, :128] / den).astype(BF)
            return carry

        lax.fori_loop(0, 4, tile, 0)

    UP, LOW = 0, 1
    at_half = {("n", LOW): 0, ("p", UP): 1, ("f", UP): 2, ("f", LOW): 3, ("n", UP): 4, ("p", LOW): 5, ("o", UP): 6, ("o", LOW): 7}
    ahead = {1: "n", -1: "p"}
    back = {1: "p", -1: "n"}
    via = {1: UP, -1: LOW}
    cols_of = [pl.ds(i * (D // SUB), D // SUB) for i in range(SUB)]

    def project(block):
        def cols(n, carry):
            at_n = pl.ds(pl.multiple_of(n * 512, 512), 512)
            done = mm(att[...], ow[:, at_n]).astype(BF)
            for part in (UP, LOW):
                pb1[at_half[block, part], :, at_n] = done[part * HALF : (part + 1) * HALF]
            return carry

        lax.fori_loop(0, 4, cols, 0)

    def rs_far(tag, pb, sbuf):
        for i, cols in enumerate(cols_of):
            for r in (1, -1):
                send((tag, "s", r, i), pb.at[at_half["f", via[r]], :, cols], ydev[r], sbuf.at[via[r], :, cols])

    def rs_near(tag, pb, fbuf, r):
        part = 1 - via[r]
        send((tag, "d", r), pb.at[at_half[ahead[r], part]], ydev[r], fbuf.at[part, via[r]])

    def rs_relay(tag, pb, sbuf, fbuf, r, i):
        cols, part = cols_of[i], via[r]
        j = at_half[ahead[r], part]
        recv((tag, "s", r, i), sbuf.at[part, :, cols])
        pb[j, :, cols] = (pb[j, :, cols].astype(F32) + sbuf[part, :, cols].astype(F32)).astype(BF)
        send((tag, "r", r, i), pb.at[j, :, cols], ydev[r], fbuf.at[part, via[r], :, cols])

    def rs_sum(tag, pb, fbuf, part, i=None):
        r = 1 if part == UP else -1
        if not i:
            recv((tag, "d", -r), fbuf.at[part, via[-r]])
        for k, cols in enumerate(cols_of):
            if i is None or i == k:
                recv((tag, "r", r, k), fbuf.at[part, via[r], :, cols])
        cols = slice(None) if i is None else cols_of[i]
        own = pb[at_half["o", part], :, cols].astype(F32)
        return own + fbuf[part, 0, :, cols].astype(F32) + fbuf[part, 1, :, cols].astype(F32)

    ynext = {"f": (y + 2) % NY, "n": (y + 1) % NY, "p": (y + NY - 1) % NY, "o": y}

    def normalise(part):
        rows = pl.ds(part * HALF, HALF)
        total = st[rows, :].astype(F32) + rs_sum("r1", pb1, f1, part)
        mixed[rows, :] = total.astype(BF)
        wide = mixed[rows, :].astype(F32)
        scale = lax.rsqrt(jnp.mean(wide * wide, axis=1, keepdims=True) + 1e-06)
        xs[at_half["o", part]] = (wide * scale * gain[...]).astype(BF)

    def g_cols(part):
        return cols_of if part == LOW else [pl.ds(0, D)]

    def g_send(part):
        for i, cols in enumerate(g_cols(part)):
            for r in (1, -1):
                send(("g", r, part, i), xs.at[at_half["o", part], :, cols], ydev[r], xs.at[at_half[back[r], part], :, cols])

    def g_recv(part, i):
        cols = g_cols(part)[i]
        for r in (1, -1):
            ref = xs.at[at_half[back[r], part], :, cols]
            recv(("g", r, part, i), ref)
            if via[r] == part:
                send(("gh", r, i), ref, ydev[r], xs.at[at_half["f", part], :, cols])

    def g_far():
        for r in (1, -1):
            for i, cols in enumerate(g_cols(via[r])):
                recv(("gh", r, i), xs.at[at_half["f", via[r]], :, cols])

    def feed(first, count):
        many = count * HALF
        rows = pl.ds(0, many)

        def cols(n, carry):
            gu = []
            for base in (0, GB):
                w = wb[:, :, :, :, pl.ds(pl.multiple_of(base + n * 256, 256), 256)].reshape(D, 256)
                gu.append(mm(xs[first : first + count].reshape(many, D), w))
            hid[rows, pl.ds(pl.multiple_of(n * 256, 256), 256)] = (gu[0] / (1.0 + jnp.exp(-gu[0])) * gu[1]).astype(BF)
            return carry

        lax.fori_loop(0, GB // 256, cols, 0, unroll=True)
        gu = mm(xs[first : first + count].reshape(many, D), wa[:, :, :, :, : 2 * rest].reshape(D, 2 * rest))
        gate, upward = gu[:, :rest], gu[:, rest:]
        hid[rows, GB:] = (gate / (1.0 + jnp.exp(-gate)) * upward).astype(BF)

        def down(n, carry):
            w = wa[pl.ds(2 * n, 2), :, :, :, 2 * rest :].reshape(512, FFL)
            at_n = pl.ds(pl.multiple_of(n * 512, 512), 512)
            pb2[first : first + count, :, at_n] = nt(hid[rows, :], w).astype(BF).reshape(count, HALF, 512)
            return carry

        lax.fori_loop(0, D // 512, down, 0)

    def near2():
        rs_near("r2", pb2, f2, 1)
        rs_near("r2", pb2, f2, -1)

    def relay2(i):
        for r in (1, -1):
            rs_relay("r2", pb2, s2, f2, r, i)

    def attend_on(block):
        if block == "o":
            loads["st"].wait()
        attend(ynext[block])

    def project_on(block):
        if block == "f":
            loads["ow"].wait()
        project(block)
        if block == "f":
            rs_far("r1", pb1, s1)
        if block == "p":
            rs_near("r1", pb1, f1, -1)

    def norm_on(part):
        normalise(part)
        g_send(part)

    steps = {
        "begin": begin,
        "turn_q": turn_q,
        "prepare": prepare,
        "near+": lambda: rs_near("r1", pb1, f1, 1),
        "norm_U": lambda: norm_on(UP),
        "norm_L": lambda: norm_on(LOW),
        "gU": lambda: g_recv(UP, 0),
        "gL0": lambda: g_recv(LOW, 0),
        "gL1": lambda: g_recv(LOW, 1),
        "ax_mid": ax_mid,
        "ax_end": ax_end,
        "feed1": lambda: (mates(), feed(0, 2), near2()),
        "feed2": lambda: (g_far(), feed(2, 2), rs_far("r2", pb2, s2)),
        "feed3": lambda: feed(4, 4),
        "r2l0": lambda: relay2(0),
        "r2l1": lambda: relay2(1),
        "fin0": lambda: finish(0),
        "fin1": lambda: finish(1),
    }

    def run_steps(name):
        if name in steps:
            return steps[name]()
        head, *rest_of = name.split("_")
        if head == "att":
            return attend_on(rest_of[0])
        if head == "proj":
            return project_on(rest_of[0])
        if head[:2] == "rl":
            return rs_relay("r1", pb1, s1, f1, 1 if head[2] == "+" else -1, int(head[3]))
        numbers = [int(n) for n in rest_of]
        return {"bz": bz, "bm": bx_mid, "be": bx_end, "az": az}[head](*numbers)

    def finish(i):
        cols = cols_of[i]
        for part in (UP, LOW):
            rows = pl.ds(part * HALF, HALF)
            out[rows, cols] = mixed[rows, cols].astype(F32) + 0.5 * rs_sum("r2", pb2, f2, part, i)

    for name in ORDER:
        run_steps(name)

    def drain():
        for cp in sent:
            cp.wait_send()

    drain()
    assert len(slots) <= NSEM


def local(queries, keys, values, sink, stream, out_weight, norm_gain, gate_weight, up_weight, down_weight):
    hbm = pl.BlockSpec(memory_space=pl.ANY)
    vmem = pl.BlockSpec(memory_space=pltpu.VMEM)
    smem = pl.BlockSpec(memory_space=pltpu.SMEM)
    V = pltpu.VMEM
    done = pl.pallas_call(
        kernel,
        name="layer",
        out_shape=jax.ShapeDtypeStruct((BLK, D), F32),
        in_specs=[hbm, hbm, hbm, smem, hbm, hbm, vmem, hbm, hbm, hbm, hbm],
        out_specs=vmem,
        scratch_shapes=[
            V((NZ, NX, NC, ROWS, CA), BF),
            V((NZ, NX, NC, ROWS, CB), BF),
            V((2 * EXT + 2 * NZ * NX * NC, 128), F32),
            V((TOK, 512), BF),
            V((4, TOK, 128), BF),
            V((2, EXT, 128), BF),
            V((4, PAD, 128), BF),
            V((4, PAD, 256), BF),
            V((512, D), BF),
            V((BLK, D), BF),
            V((BLK, QW), F32),
            V((BLK, 512), BF),
            V((8, HALF, D), BF),
            V((2, HALF, D), BF),
            V((2, 2, HALF, D), BF),
            V((8, HALF, D), BF),
            V((2, HALF, D), BF),
            V((2, 2, HALF, D), BF),
            V((BLK, D), BF),
            V((8, HALF, D), BF),
            V((2 * BLK, FFL), BF),
            pltpu.SemaphoreType.DMA((11,)),
            pltpu.SemaphoreType.DMA((NSEM,)),
            pltpu.SemaphoreType.DMA((NSEM,)),
        ],
        compiler_params=pltpu.CompilerParams(
            collective_id=0, has_side_effects=True, vmem_limit_bytes=62 * 1024 * 1024
        ),
    )(
        queries, keys, values, sink, stream, out_weight, norm_gain.reshape(1, D),
        gate_weight, up_weight, down_weight.T, jnp.asarray(tables()),
    )
    return done.astype(BF)


def solution(mesh):
    placed = (
        P("sp", "tp"), P("sp", "tp"), P("sp", "tp"), P("tp"), P(("sp", "tp"), None), P("tp", None), P(),
        P("sp", "tp"), P("sp", "tp"), P("tp", "sp"),
    )
    return jax.shard_map(local, mesh=mesh, in_specs=placed, out_specs=P(("sp", "tp"), None), check_vma=False)
```

time: 110 us -> 95.7 us (0.87)
  Pallas kernels: 106 us -> 93.3 us
  local copies, waits for them, and re-layouts: 3.78 us -> 0 us
  other arithmetic: 0 us -> 2.24 us
    pallas_call x1, Pallas kernels: 106 us -> 93.3 us  [local(): pl.pallas_call(kernel, name='layer', out_shape=jax.ShapeDtypeStruct((BLK,...]
    unnamed x2 -> x0, local copies, waits for them, and re-layouts: 3.78 us -> none
    convert_element_type x0 -> x1, other arithmetic: none -> 2.24 us  [local(): return done.astype(BF)]
where the time goes in v2:
time: 95.7 us; the launch traced here: 95.5 us
  Pallas kernels  93.3 us (97%)
  other arithmetic  2.24 us (2%)
    pallas_call x1, Pallas kernels, local(): pl.pallas_call(kernel, name='layer', out_shape=jax.ShapeDtypeStruct((BLK,...  93.3 us
    convert_element_type x1, other arithmetic, local(): return done.astype(BF)  2.24 us

profile of v2, /device:TPU:1, one launch (start us, length us, event | category | flops | bytes accessed | tf_op | source)
XLA Modules:
  0.0 95.5 jit_solution(5352408152925782444)
XLA Ops:
  0.0 93.3 %layer.1 = f32[160,2048]{1,0:T(8,128)} custom-call(bf16[640,512]{1,0:T(8,128)(2,1)} %q_hbm.1, bf16[640,128]{1,0:T(8,128)(2,1)} %k_hbm.1, bf16[640,128]{1,0:T(8,128)(2,1)} %v_hbm.1, f32[8]{0:T(128)} %sink.1, bf16[160,2048]{1,0:T(8,128)(2,1)} %st_hbm.1, bf16[512,2048]{1,0:T(8,128)(2,1)} %ow_hbm.1, f32[1,2048]{1,0:T(1,128)} %bitcast.3, bf16[32,1408]{1,0:T(8,128)(2,1)} %g_hbm.1, ...), custom_call_target="tpu_custom_call" | custom-call | tf_op jit(solution)/shard_map/layer/pallas_call | solution.py:482
  93.3 2.2 %convert_element_type.3 = bf16[160,2048]{1,0:T(8,128)(2,1)} convert(f32[160,2048]{1,0:T(8,128)} %layer.1) | non-fusion elementwise | flops 327680 | bytes 1966080 | tf_op jit(solution)/shard_map/convert_element_type | solution.py:521

commit v3 on v2

v3 whole, which is shorter than its diff:
```python
import jax
import jax.numpy as jnp
import numpy as np
from jax import lax
from jax.experimental import pallas as pl
from jax.experimental.pallas import tpu as pltpu
from jax.sharding import PartitionSpec as P

HEAD = 64
WINDOW = 128
MESH = pl.DeviceIdType.MESH
BF = jnp.bfloat16
F32 = jnp.float32

NZ, NX, NC, NY = 8, 4, 2, 4
ROWS = 32
TOK = 640
BLK = TOK // NY
HALF = BLK // 2
EXT = TOK + 2 * WINDOW
PAD = 3 * BLK + 4 * WINDOW
D = 2048
FFL = 1408
GB = 1280
CB = 2 * GB
CA = 2 * (FFL - GB) + FFL
QW = 512
NRECV = 62
NSEND = 14
ORDER = (
    "begin", "turn_q", "prep_own", "prepare", "att_f", "bz_1", "proj_f", "ax_mid", "bm_0", "az_1_0", "att_n",
    "proj_n", "att_p", "rl+0", "bz_2", "proj_p", "rl-0", "att_o", "rl+1", "near+", "rl-1", "proj_o", "ax_end",
    "bm_1", "az_1_1", "bm_-1", "az_1_-1", "az_2_0", "be_0", "tr_0", "bm_2", "bz_3", "norm_U", "az_1_2", "bm_-2",
    "tr_1", "tr_-1", "az_2_1", "be_1", "be_-1", "az_2_-1", "be_2", "norm_L", "az_3_0", "bz_4", "bm_3", "az_2_2",
    "tr_2", "tr_-2", "bm_-3", "az_3_1", "gU", "be_-2", "az_3_-1", "az_4_0", "gL0", "bm_4", "az_3_2", "az_4_1",
    "be_3", "tr_3", "tr_-3", "gL1", "az_4_-1", "be_-3", "az_4_2", "be_4", "tr_4", "feed1", "near0", "near1", "feed2",
    "feed3", "r2l0", "r2l1", "fin0", "fin1",
)
SUB = 2


def tables():
    lane = (np.arange(128) % 64) % 32
    freq = 1.0 / 10000.0 ** (2.0 * lane / HEAD)
    near = (np.arange(EXT) - WINDOW)[:, None] * freq[None]
    far = (np.arange(NZ * NX * NC) * TOK)[:, None] * freq[None]
    return np.concatenate([np.cos(near), np.sin(near), np.cos(far), np.sin(far)], 0).astype(np.float32)


def nt(a, b):
    return lax.dot_general(a, b, (((1,), (1,)), ((), ())), preferred_element_type=F32)


def mm(a, b):
    return jnp.dot(a, b, preferred_element_type=F32)


def kernel(
    q_hbm, k_hbm, v_hbm, sink, st_hbm, ow_hbm, gain, g_hbm, u_hbm, d_hbm, tab_hbm,
    out,
    wa, wb, tab, q, qr, kv, kk, vv, ow, st, bias, att,
    pb1, s1, f1, pb2, s2, f2, mixed, xs, hid, dt,
    lsem, ssem, rsem,
):
    s = lax.axis_index("sp")
    y = lax.axis_index("tp")
    c = s % NC
    x = (s // NC) % NX
    z = s // (NC * NX)

    def at(zz, xx, cc):
        return ((zz % NZ) * NX + xx % NX) * NC + cc

    ydev = {1: (s, (y + 1) % NY), -1: (s, (y + NY - 1) % NY)}
    xdev = {1: (at(z, x + 1, c), y), -1: (at(z, x + NX - 1, c), y)}
    zdev = {1: (at(z + 1, x, c), y), -1: (at(z + NZ - 1, x, c), y)}
    mate = (at(z, x, 1 - c), y)
    nsp = NZ * NX * NC
    hdev = {1: ((s + 1) % nsp, y), -1: ((s + nsp - 1) % nsp, y)}

    barrier = pltpu.get_barrier_semaphore()
    for dev in (*ydev.values(), *xdev.values(), *zdev.values(), mate, *hdev.values()):
        pl.semaphore_signal(barrier, inc=1, device_id=dev, device_id_type=MESH)

    loads = {}

    def load(name, src, dst):
        i = loads.setdefault(name, len(loads))
        pltpu.make_async_copy(src, dst, lsem.at[i]).start()

    def loaded(name, ref):
        pltpu.make_async_copy(ref, ref, lsem.at[loads[name]]).wait()

    rest = FFL - GB
    load("kv", k_hbm, kv.at[0, pl.ds(WINDOW, TOK)])
    load("kv", v_hbm, kv.at[1, pl.ds(WINDOW, TOK)])
    load("b", g_hbm.at[:, pl.ds(0, GB)], wb.at[z, x, c, :, pl.ds(0, GB)])
    load("b", u_hbm.at[:, pl.ds(0, GB)], wb.at[z, x, c, :, pl.ds(GB, GB)])
    load("a", d_hbm, wa.at[z, x, c, :, pl.ds(2 * rest, FFL)])
    load("a", g_hbm.at[:, pl.ds(GB, rest)], wa.at[z, x, c, :, pl.ds(0, rest)])
    load("a", u_hbm.at[:, pl.ds(GB, rest)], wa.at[z, x, c, :, pl.ds(rest, rest)])
    load("tab", tab_hbm, tab)
    load("q", q_hbm, q)
    load("ow", ow_hbm, ow)
    load("st", st_hbm, st)

    def greet():
        pl.semaphore_wait(barrier, 9)

    greet()

    taken, given = {}, {}

    def send(key, kind, ref, dev, dst=None):
        i = taken.setdefault(key, len(taken))
        k = given.setdefault(kind, len(given))
        pltpu.make_async_remote_copy(
            src_ref=ref, dst_ref=ref if dst is None else dst, send_sem=ssem.at[k], recv_sem=rsem.at[i],
            device_id=dev, device_id_type=MESH,
        ).start()

    def recv(key, ref):
        i = taken.setdefault(key, len(taken))
        pltpu.make_async_copy(ref, ref, rsem.at[i]).wait()

    def zb(dz, half=None):
        ref = wb.at[(z + dz + NZ) % NZ, x, c]
        return ref if half is None else ref.at[pl.ds(16 * half, 16)]

    def xb(dz, dx, half=None):
        ref = wb.at[(z + dz + NZ) % NZ, (x + dx + NX) % NX, c]
        return ref if half is None else ref.at[pl.ds(16 * half, 16)]

    def za(dz, dx, half=None):
        ref = wa.at[(z + dz + NZ) % NZ, (x + dx + NX) % NX, c]
        return ref if half is None else ref.at[pl.ds(16 * half, 16)]

    def xa(dx, half=None):
        ref = wa.at[z, (x + dx + NX) % NX, c]
        return ref if half is None else ref.at[pl.ds(16 * half, 16)]

    oneb, onea = wb.at[0, 0, 0], wa.at[0, 0, 0]
    twob, twoa = wb.at[pl.ds(0, 2), 0, 0], wa.at[pl.ds(0, 2), 0, 0]
    way = ((1, 0), (-1, 1))

    def b_mate(dz, dx):
        send(("bm",), "bm", xb(dz, dx), mate)

    def a_mate(dz, dx):
        send(("am", dz), "am", za(dz, dx), mate)

    def bx_send(dz):
        for r in (1, -1):
            send(("bx", dz), "bx", xb(dz, 0), xdev[r])
        b_mate(dz, 0)

    def bx_mid(dz):
        recv(("bx", dz), twob)
        for r, half in way:
            send(("bh", dz), "bh", xb(dz, -r, half), xdev[r])
        for r in (1, -1):
            b_mate(dz, r)

    def bx_end(dz):
        recv(("bh", dz), oneb)
        b_mate(dz, 2)

    def bz(n):
        recv(("bz", n), twob if n < 4 else oneb)
        for r, half in way:
            if n < 3:
                send(("bz", n + 1), "bz", zb(-r * n), zdev[r])
            elif n == 3:
                send(("bz", 4), "bzh", zb(-r * 3, half), zdev[r])
        for dz in (n, -n) if n < 4 else (4,):
            bx_send(dz)

    def az_send(n, dx, r):
        if n < 4:
            send(("az", n, dx), "az", za(-r * (n - 1), dx), zdev[r])
        else:
            send(("az", 4, dx), "azh", za(-r * 3, dx, 0 if r == 1 else 1), zdev[r])

    def az(n, dx):
        recv(("az", n, dx), twoa if n < 4 else onea)
        for r in (1, -1):
            if n < 4:
                az_send(n + 1, dx, r)
        for dz in (n, -n) if n < 4 else (4,):
            a_mate(dz, dx)

    def ax_mid():
        recv(("ax",), twoa)
        for r, half in way:
            send(("ah",), "ah", xa(-r, half), xdev[r])
        for r in (1, -1):
            for dx in (1, -1):
                az_send(1, dx, r)
        for r in (1, -1):
            a_mate(0, r)

    def ax_end():
        recv(("ah",), onea)
        for r in (1, -1):
            az_send(1, 2, r)
        a_mate(0, 2)

    def turn_down(dz):
        zz = (z + dz + NZ) % NZ
        recv(("am", dz), wa.at[0, :, 0])
        dt[:, pl.ds(pl.multiple_of(zz * 256, 256), 256)] = wa[zz, :, :, :, 2 * rest :].reshape(256, FFL).T

    def mates():
        recv(("bm",), wb.at[:, :, 0])

    def begin():
        loaded("kv", kv.at[:, pl.ds(0, TOK)])
        send(("halo",), "halo", kv.at[:, pl.ds(WINDOW, WINDOW)], hdev[-1], kv.at[:, pl.ds(WINDOW + TOK, WINDOW)])
        send(("halo",), "halo", kv.at[:, pl.ds(TOK, WINDOW)], hdev[1], kv.at[:, pl.ds(0, WINDOW)])
        loaded("b", oneb)
        loaded("a", onea)
        for r in (1, -1):
            send(("bz", 1), "bz", zb(0), zdev[r])
            send(("ax",), "ax", xa(0), xdev[r])
        for r in (1, -1):
            az_send(1, 0, r)
        bx_send(0)
        a_mate(0, 0)

    loaded("tab", tab)
    cb = tab[pl.ds(2 * EXT + s, 1), :]
    sb = tab[pl.ds(2 * EXT + nsp + s, 1), :]

    def rotate(rows, value):
        cl, sl = tab[rows, :], tab[pl.ds(EXT + rows.start, rows.size), :]
        cos = cb * cl - sb * sl
        sin = sb * cl + cb * sl
        return value.astype(F32) * cos + mm(value, turn) * sin

    jj = lax.broadcasted_iota(jnp.int32, (128, 128), 0)
    ii = lax.broadcasted_iota(jnp.int32, (128, 128), 1)
    low = (ii % 64) < 32
    turn = (jnp.where(jj == ii - 32, jnp.where(low, 0.0, 1.0), 0.0)
            - jnp.where(jj == ii + 32, jnp.where(low, 1.0, 0.0), 0.0)).astype(BF)
    flip = jnp.where((jj + 64) % 128 == ii, 1.0, 0.0).astype(BF)

    def turn_q():
        loaded("q", q)
        for t in range(4):
            qr[t] = rotate(pl.ds(WINDOW, TOK), q[:, 128 * t : 128 * (t + 1)]).astype(BF)

    def prepare(first, many):
        rows = pl.ds(first, many)
        lane = lax.broadcasted_iota(jnp.int32, (many, 128), 1)
        left = lane < 64
        kr = rotate(rows, kv[0, rows]).astype(BF)
        ks = mm(kr, flip)
        kr = kr.astype(F32)
        vr = kv[1, rows].astype(F32)
        vs = mm(kv[1, rows], flip)
        for i in range(4):
            ksrc, vsrc = ((kr, vr), (ks, vs), (ks, vs), (kr, vr))[i]
            keep = left if i % 2 == 0 else lane >= 64
            kk[i, rows, :] = jnp.where(keep, ksrc, 0.0).astype(BF)
            vv[i, rows, :128] = jnp.where(keep, vsrc, 0.0).astype(BF)

    def prepare_own():
        left = lax.broadcasted_iota(jnp.int32, (EXT, 128), 1) < 64
        one = jnp.where(left, 1.0, 0.0).astype(BF)
        two = jnp.where(left, 0.0, 1.0).astype(BF)
        for i in range(4):
            kk[i, EXT:, :] = jnp.zeros((PAD - EXT, 128), BF)
            vv[i, EXT:, :] = jnp.zeros((PAD - EXT, 256), BF)
            vv[i, :EXT, 128:] = one if i % 2 == 0 else two
        prepare(WINDOW, TOK)

    def prepare_ends():
        recv(("halo",), kv.at[:, pl.ds(0, 2 * WINDOW)])
        prepare(0, WINDOW)
        prepare(WINDOW + TOK, WINDOW)

    def attend(b):
        first = s * TOK + b * BLK
        ri = lax.broadcasted_iota(jnp.int32, (BLK, QW), 0)
        ci = lax.broadcasted_iota(jnp.int32, (BLK, QW), 1)
        lo = jnp.maximum(ri, WINDOW - first)
        hi = jnp.minimum(ri + 2 * WINDOW, nsp * TOK - 1 + WINDOW - first)
        bias[...] = jnp.where((ci >= lo) & (ci <= hi), 0.0, -jnp.inf)
        rows = pl.multiple_of(b * BLK, 32)
        half = lax.broadcasted_iota(jnp.int32, (BLK, 128), 1) < 64

        def tile(t, carry):
            qt = qr[t, pl.ds(rows, BLK), :]
            acc, ends = None, []
            for par in range(2):
                i = (t // 2) * 2 + par
                sc = nt(qt, kk[i, pl.ds(rows, QW), :]) * 0.125 + bias[...]
                snk = sink[2 * t + par]
                top = jnp.maximum(jnp.max(sc, axis=1, keepdims=True), snk)
                prob = jnp.exp(sc - top).astype(BF)
                part = mm(prob, vv[i, pl.ds(rows, QW), :])
                acc = part if acc is None else acc + part
                ends.append(jnp.exp(snk - top))
            den = acc[:, 128:] + jnp.where(half, ends[0], ends[1])
            att[:, pl.ds(pl.multiple_of(t * 128, 128), 128)] = (acc[:, :128] / den).astype(BF)
            return carry

        lax.fori_loop(0, 4, tile, 0, unroll=True)

    UP, LOW = 0, 1
    at_half = {("n", LOW): 0, ("p", UP): 1, ("f", UP): 2, ("f", LOW): 3, ("n", UP): 4, ("p", LOW): 5, ("o", UP): 6, ("o", LOW): 7}
    ahead = {1: "n", -1: "p"}
    back = {1: "p", -1: "n"}
    via = {1: UP, -1: LOW}
    cols_of = [pl.ds(i * (D // SUB), D // SUB) for i in range(SUB)]

    def project(block):
        def cols(n, carry):
            at_n = pl.ds(pl.multiple_of(n * 512, 512), 512)
            done = mm(att[...], ow[:, at_n]).astype(BF)
            for part in (UP, LOW):
                pb1[at_half[block, part], :, at_n] = done[part * HALF : (part + 1) * HALF]
            return carry

        lax.fori_loop(0, 4, cols, 0)

    def rs_far(tag, pb, sbuf):
        for i, cols in enumerate(cols_of):
            for r in (1, -1):
                key = (tag, "s", i) if tag == "r2" else (tag, "s", r, i)
                send(key, tag, pb.at[at_half["f", via[r]], :, cols], ydev[r], sbuf.at[via[r], :, cols])

    def sum_key(tag, part, i):
        return (tag, "f", i if tag == "r2" else part)

    def rs_near(tag, pb, fbuf, r, i):
        part, cols = 1 - via[r], cols_of[i]
        send(sum_key(tag, part, i), tag, pb.at[at_half[ahead[r], part], :, cols], ydev[r], fbuf.at[part, via[r], :, cols])

    def rs_relay(tag, pb, sbuf, fbuf, r, i):
        cols, part = cols_of[i], via[r]
        j = at_half[ahead[r], part]
        if tag == "r1":
            recv((tag, "s", r, i), sbuf.at[part, :, cols])
        pb[j, :, cols] = (pb[j, :, cols].astype(F32) + sbuf[part, :, cols].astype(F32)).astype(BF)
        send(sum_key(tag, part, i), tag, pb.at[j, :, cols], ydev[r], fbuf.at[part, via[r], :, cols])

    def rs_sum(pb, fbuf, part, cols):
        own = pb[at_half["o", part], :, cols].astype(F32)
        return own + fbuf[part, 0, :, cols].astype(F32) + fbuf[part, 1, :, cols].astype(F32)

    ynext = {"f": (y + 2) % NY, "n": (y + 1) % NY, "p": (y + NY - 1) % NY, "o": y}

    def normalise(part):
        rows = pl.ds(part * HALF, HALF)
        recv(sum_key("r1", part, 0), pb1.at[pl.ds(0, 2)])
        total = st[rows, :].astype(F32) + rs_sum(pb1, f1, part, slice(None))
        mixed[rows, :] = total.astype(BF)
        wide = mixed[rows, :].astype(F32)
        scale = lax.rsqrt(jnp.mean(wide * wide, axis=1, keepdims=True) + 1e-06)
        xs[at_half["o", part]] = (wide * scale * gain[...]).astype(BF)

    def g_cols(part):
        return cols_of if part == LOW else [pl.ds(0, D)]

    def g_send(part):
        for i, cols in enumerate(g_cols(part)):
            for r in (1, -1):
                send(("g", part, i), "g", xs.at[at_half["o", part], :, cols], ydev[r], xs.at[at_half[back[r], part], :, cols])

    def g_recv(part, i):
        cols = g_cols(part)[i]
        recv(("g", part, i), xs.at[pl.ds(0, 2), :, cols])
        for r in (1, -1):
            if via[r] == part:
                ref = xs.at[at_half[back[r], part], :, cols]
                send(("gh",), "g", ref, ydev[r], xs.at[at_half["f", part], :, cols])

    def g_far():
        recv(("gh",), xs.at[pl.ds(0, 2)])

    def gate_up(first, count):
        many = count * HALF
        rows = pl.ds(0, many)

        def act(gate, upward):
            return (gate / (1.0 + jnp.exp(-gate)) * upward).astype(BF)

        def cols(n, carry):
            gu = []
            for base in (0, GB):
                w = wb[:, :, :, :, pl.ds(pl.multiple_of(base + n * 256, 256), 256)].reshape(D, 256)
                gu.append(mm(xs[first : first + count].reshape(many, D), w))
            hid[rows, pl.ds(pl.multiple_of(n * 256, 256), 256)] = act(*gu)
            return carry

        gu = mm(xs[first : first + count].reshape(many, D), wa[:, :, :, :, : 2 * rest].reshape(D, 2 * rest))
        hid[rows, GB:] = act(gu[:, :rest], gu[:, rest:])
        lax.fori_loop(0, GB // 256, cols, 0, unroll=True)

    def down(first, count, i):
        many = count * HALF

        def cols(n, carry):
            at_n = pl.ds(pl.multiple_of(i * (D // SUB) + n * 512, 512), 512)
            done = mm(hid[pl.ds(0, many), :], dt[:, at_n]).astype(BF)
            pb2[first : first + count, :, at_n] = done.reshape(count, HALF, 512)
            return carry

        lax.fori_loop(0, D // SUB // 512, cols, 0, unroll=True)

    def near2(i):
        down(0, 2, i)
        for r in (1, -1):
            rs_near("r2", pb2, f2, r, i)

    def far2():
        g_far()
        gate_up(2, 2)
        for i in range(SUB):
            down(2, 2, i)
        rs_far("r2", pb2, s2)

    def own2():
        gate_up(4, 4)
        for i in range(SUB):
            down(4, 4, i)

    def first2():
        mates()
        gate_up(0, 2)

    def near1(r):
        for i in range(SUB):
            rs_near("r1", pb1, f1, r, i)

    def relay2(i):
        recv(("r2", "s", i), s2.at[:, :, cols_of[i]])
        for r in (1, -1):
            rs_relay("r2", pb2, s2, f2, r, i)

    def attend_on(block):
        if block == "o":
            loaded("st", st)
        attend(ynext[block])

    def project_on(block):
        if block == "f":
            loaded("ow", ow)
        project(block)
        if block == "f":
            rs_far("r1", pb1, s1)
        if block == "p":
            near1(-1)

    def norm_on(part):
        normalise(part)
        g_send(part)

    steps = {
        "begin": begin,
        "turn_q": turn_q,
        "prep_own": prepare_own,
        "prepare": prepare_ends,
        "near+": lambda: near1(1),
        "norm_U": lambda: norm_on(UP),
        "norm_L": lambda: norm_on(LOW),
        "gU": lambda: g_recv(UP, 0),
        "gL0": lambda: g_recv(LOW, 0),
        "gL1": lambda: g_recv(LOW, 1),
        "ax_mid": ax_mid,
        "ax_end": ax_end,
        "feed1": first2,
        "near0": lambda: near2(0),
        "near1": lambda: near2(1),
        "feed2": far2,
        "feed3": own2,
        "r2l0": lambda: relay2(0),
        "r2l1": lambda: relay2(1),
        "fin0": lambda: finish(0),
        "fin1": lambda: finish(1),
    }

    def run_steps(name):
        if name in steps:
            return steps[name]()
        head, *rest_of = name.split("_")
        if head == "att":
            return attend_on(rest_of[0])
        if head == "proj":
            return project_on(rest_of[0])
        if head[:2] == "rl":
            return rs_relay("r1", pb1, s1, f1, 1 if head[2] == "+" else -1, int(head[3]))
        numbers = [int(n) for n in rest_of]
        return {"bz": bz, "bm": bx_mid, "be": bx_end, "az": az, "tr": turn_down}[head](*numbers)

    def finish(i):
        cols = cols_of[i]
        recv(("r2", "f", i), pb2.at[pl.ds(0, 2)])
        for part in (UP, LOW):
            rows = pl.ds(part * HALF, HALF)
            out[rows, cols] = mixed[rows, cols].astype(F32) + 0.5 * rs_sum(pb2, f2, part, cols)

    for name in ORDER:
        run_steps(name)

    def drain():
        everything = {
            "halo": kv.at[:, pl.ds(0, 2 * WINDOW)],
            "bz": wb.at[pl.ds(0, 6), 0, 0], "bzh": oneb, "bx": wb.at[:, pl.ds(0, 2), 0], "bh": wb.at[:, 0, 0],
            "bm": wb.at[:, :, 0], "ax": twoa, "ah": onea, "az": wa.at[pl.ds(0, 6), :, 0], "azh": wa.at[0, :, 0],
            "am": wa.at[:, :, 0], "r1": pb1.at[pl.ds(0, 6)], "r2": pb2.at[pl.ds(0, 6)], "g": xs.at[pl.ds(0, 6)],
        }
        for kind, ref in everything.items():
            pltpu.make_async_copy(ref, ref, ssem.at[given[kind]]).wait()

    drain()
    assert len(taken) == NRECV and len(given) == NSEND, (len(taken), len(given))


def local(queries, keys, values, sink, stream, out_weight, norm_gain, gate_weight, up_weight, down_weight):
    hbm = pl.BlockSpec(memory_space=pl.ANY)
    vmem = pl.BlockSpec(memory_space=pltpu.VMEM)
    smem = pl.BlockSpec(memory_space=pltpu.SMEM)
    V = pltpu.VMEM
    done = pl.pallas_call(
        kernel,
        name="layer",
        out_shape=jax.ShapeDtypeStruct((BLK, D), F32),
        in_specs=[hbm, hbm, hbm, smem, hbm, hbm, vmem, hbm, hbm, hbm, hbm],
        out_specs=vmem,
        scratch_shapes=[
            V((NZ, NX, NC, ROWS, CA), BF),
            V((NZ, NX, NC, ROWS, CB), BF),
            V((2 * EXT + 2 * NZ * NX * NC, 128), F32),
            V((TOK, 512), BF),
            V((4, TOK, 128), BF),
            V((2, EXT, 128), BF),
            V((4, PAD, 128), BF),
            V((4, PAD, 256), BF),
            V((512, D), BF),
            V((BLK, D), BF),
            V((BLK, QW), F32),
            V((BLK, 512), BF),
            V((8, HALF, D), BF),
            V((2, HALF, D), BF),
            V((2, 2, HALF, D), BF),
            V((8, HALF, D), BF),
            V((2, HALF, D), BF),
            V((2, 2, HALF, D), BF),
            V((BLK, D), BF),
            V((8, HALF, D), BF),
            V((2 * BLK, FFL), BF),
            V((FFL, D), BF),
            pltpu.SemaphoreType.DMA((7,)),
            pltpu.SemaphoreType.DMA((NSEND,)),
            pltpu.SemaphoreType.DMA((NRECV,)),
        ],
        compiler_params=pltpu.CompilerParams(
            collective_id=0, has_side_effects=True, vmem_limit_bytes=62 * 1024 * 1024
        ),
    )(
        queries, keys, values, sink, stream, out_weight, norm_gain.reshape(1, D),
        gate_weight, up_weight, down_weight.T, jnp.asarray(tables()),
    )
    return done.astype(BF)


def solution(mesh):
    placed = (
        P("sp", "tp"), P("sp", "tp"), P("sp", "tp"), P("tp"), P(("sp", "tp"), None), P("tp", None), P(),
        P("sp", "tp"), P("sp", "tp"), P("tp", "sp"),
    )
    return jax.shard_map(local, mesh=mesh, in_specs=placed, out_specs=P(("sp", "tp"), None), check_vma=False)
```

time: 95.7 us -> 90.4 us (0.945)
  Pallas kernels: 93.3 us -> 88 us
    pallas_call x1, Pallas kernels: 93.3 us -> 88 us  [local(): pl.pallas_call(kernel, name='layer', out_shape=jax.ShapeDtypeStruct((BLK,...]
where the time goes in v3:
time: 90.4 us; the launch traced here: 90.2 us
  Pallas kernels  88 us (97%)
  other arithmetic  2.24 us (2%)
    pallas_call x1, Pallas kernels, local(): pl.pallas_call(kernel, name='layer', out_shape=jax.ShapeDtypeStruct((BLK,...  88 us
    convert_element_type x1, other arithmetic, local(): return done.astype(BF)  2.24 us

profile of v3, /device:TPU:1, one launch (start us, length us, event | category | flops | bytes accessed | tf_op | source)
XLA Modules:
  0.0 90.2 jit_solution(7795208438239189790)
XLA Ops:
  0.0 88.0 %layer.1 = f32[160,2048]{1,0:T(8,128)} custom-call(bf16[640,512]{1,0:T(8,128)(2,1)} %q_hbm.1, bf16[640,128]{1,0:T(8,128)(2,1)} %k_hbm.1, bf16[640,128]{1,0:T(8,128)(2,1)} %v_hbm.1, f32[8]{0:T(128)} %sink.1, bf16[160,2048]{1,0:T(8,128)(2,1)} %st_hbm.1, bf16[512,2048]{1,0:T(8,128)(2,1)} %ow_hbm.1, f32[1,2048]{1,0:T(1,128)} %bitcast.3, bf16[32,1408]{1,0:T(8,128)(2,1)} %g_hbm.1, ...), custom_call_target="tpu_custom_call" | custom-call | tf_op jit(solution)/shard_map/layer/pallas_call | solution.py:526
  88.0 2.2 %convert_element_type.3 = bf16[160,2048]{1,0:T(8,128)(2,1)} convert(f32[160,2048]{1,0:T(8,128)} %layer.1) | non-fusion elementwise | flops 327680 | bytes 1966080 | tf_op jit(solution)/shard_map/convert_element_type | solution.py:566

commit v4 on v3

--- a/solution.py
+++ b/solution.py
@@ -25,15 +25,15 @@
 CB = 2 * GB
 CA = 2 * (FFL - GB) + FFL
 QW = 512
-NRECV = 62
+NRECV = 63
 NSEND = 14
 ORDER = (
-    "begin", "turn_q", "prep_own", "prepare", "att_f", "bz_1", "proj_f", "ax_mid", "bm_0", "az_1_0", "att_n",
-    "proj_n", "att_p", "rl+0", "bz_2", "proj_p", "rl-0", "att_o", "rl+1", "near+", "rl-1", "proj_o", "ax_end",
-    "bm_1", "az_1_1", "bm_-1", "az_1_-1", "az_2_0", "be_0", "tr_0", "bm_2", "bz_3", "norm_U", "az_1_2", "bm_-2",
-    "tr_1", "tr_-1", "az_2_1", "be_1", "be_-1", "az_2_-1", "be_2", "norm_L", "az_3_0", "bz_4", "bm_3", "az_2_2",
-    "tr_2", "tr_-2", "bm_-3", "az_3_1", "gU", "be_-2", "az_3_-1", "az_4_0", "gL0", "bm_4", "az_3_2", "az_4_1",
-    "be_3", "tr_3", "tr_-3", "gL1", "az_4_-1", "be_-3", "az_4_2", "be_4", "tr_4", "feed1", "near0", "near1", "feed2",
+    "begin", "turn_q", "prep_own", "prepare", "att_f", "proj_f", "bz_1", "att_n", "proj_n", "att_p", "az_1_0",
+    "proj_p", "ax_mid", "att_o", "rl-0", "proj_o", "bz_2", "bm_1", "rl+0", "bm_0", "az_2_0", "rl+1", "near+", "rl-1",
+    "bm_-1", "ax_end", "az_1_1", "tr_0", "az_1_-1", "bm_2", "bz_3", "norm_U", "bm_-2", "az_3_0", "be_1", "az_1_2",
+    "be_0", "tr_1", "tr_-1", "be_-1", "az_2_1", "norm_L", "be_2", "az_2_-1", "bz_4", "bm_3", "az_4_0", "az_2_2",
+    "gU", "bm_-3", "tr_2", "tr_-2", "az_3_1", "be_-2", "gL0", "az_3_-1", "bm_4", "az_3_2", "gL1", "early1", "az_4_1",
+    "be_3", "tr_3", "az_4_-1", "tr_-3", "be_-3", "az_4_2", "be_4", "tr_4", "feed1", "near0", "near1", "feed2",
     "feed3", "r2l0", "r2l1", "fin0", "fin1",
 )
 SUB = 2
@@ -56,10 +56,10 @@
 
 
 def kernel(
-    q_hbm, k_hbm, v_hbm, sink, st_hbm, ow_hbm, gain, g_hbm, u_hbm, d_hbm, tab_hbm,
+    q_hbm, k_hbm, v_hbm, sink_hbm, st_hbm, ow_hbm, gain_hbm, g_hbm, u_hbm, d_hbm, tab_hbm,
     out,
     wa, wb, tab, q, qr, kv, kk, vv, ow, st, bias, att,
-    pb1, s1, f1, pb2, s2, f2, mixed, xs, hid, dt,
+    pb1, s1, f1, pb2, s2, f2, mixed, xs, hid, dt, pre, gain, sink,
     lsem, ssem, rsem,
 ):
     s = lax.axis_index("sp")
@@ -103,6 +103,8 @@
     load("q", q_hbm, q)
     load("ow", ow_hbm, ow)
     load("st", st_hbm, st)
+    load("gain", gain_hbm, gain)
+    load("sink", sink_hbm, sink)
 
     def greet():
         pl.semaphore_wait(barrier, 9)
@@ -144,7 +146,7 @@
     way = ((1, 0), (-1, 1))
 
     def b_mate(dz, dx):
-        send(("bm",), "bm", xb(dz, dx), mate)
+        send(("bm", abs(dz) > 2), "bm", xb(dz, dx), mate)
 
     def a_mate(dz, dx):
         send(("am", dz), "am", za(dz, dx), mate)
@@ -210,8 +212,8 @@
         recv(("am", dz), wa.at[0, :, 0])
         dt[:, pl.ds(pl.multiple_of(zz * 256, 256), 256)] = wa[zz, :, :, :, 2 * rest :].reshape(256, FFL).T
 
-    def mates():
-        recv(("bm",), wb.at[:, :, 0])
+    def mates(last):
+        recv(("bm", last), wb.at[pl.ds(0, 3 if last else 5), :, 0])
 
     def begin():
         loaded("kv", kv.at[:, pl.ds(0, TOK)])
@@ -398,6 +400,38 @@
         hid[rows, GB:] = act(gu[:, :rest], gu[:, rest:])
         lax.fori_loop(0, GB // 256, cols, 0, unroll=True)
 
+    def over(n, dz):
+        zz = (z + dz + NZ) % NZ
+        act = xs[0:2, :, pl.ds(pl.multiple_of(zz * 256, 256), 256)].reshape(BLK, 256)
+        if n < CB // 256:
+            w = wb[zz, :, :, :, 256 * n : 256 * (n + 1)]
+        else:
+            w = wa[zz, :, :, :, : 2 * rest]
+        return mm(act, w.reshape(256, 256))
+
+    def early():
+        mates(False)
+        for n in range(CB // 256 + 1):
+            acc = over(n, 0)
+            for dz in (1, -1, 2, -2):
+                acc = acc + over(n, dz)
+            pre[n] = acc
+
+    def late():
+        mates(True)
+        parts_of = GB // 256
+
+        def total(n):
+            return pre[n] + over(n, 3) + over(n, -3) + over(n, 4)
+
+        def act(gate, upward):
+            return (gate / (1.0 + jnp.exp(-gate)) * upward).astype(BF)
+
+        for n in range(parts_of):
+            hid[:BLK, 256 * n : 256 * (n + 1)] = act(total(n), total(parts_of + n))
+        gu = total(2 * parts_of)
+        hid[:BLK, GB:] = act(gu[:, :rest], gu[:, rest:])
+
     def down(first, count, i):
         many = count * HALF
 
@@ -426,10 +460,6 @@
         for i in range(SUB):
             down(4, 4, i)
 
-    def first2():
-        mates()
-        gate_up(0, 2)
-
     def near1(r):
         for i in range(SUB):
             rs_near("r1", pb1, f1, r, i)
@@ -440,8 +470,11 @@
             rs_relay("r2", pb2, s2, f2, r, i)
 
     def attend_on(block):
+        if block == "f":
+            loaded("sink", sink)
         if block == "o":
             loaded("st", st)
+            loaded("gain", gain)
         attend(ynext[block])
 
     def project_on(block):
@@ -470,7 +503,8 @@
         "gL1": lambda: g_recv(LOW, 1),
         "ax_mid": ax_mid,
         "ax_end": ax_end,
-        "feed1": first2,
+        "early1": early,
+        "feed1": late,
         "near0": lambda: near2(0),
         "near1": lambda: near2(1),
         "feed2": far2,
@@ -499,7 +533,7 @@
         recv(("r2", "f", i), pb2.at[pl.ds(0, 2)])
         for part in (UP, LOW):
             rows = pl.ds(part * HALF, HALF)
-            out[rows, cols] = mixed[rows, cols].astype(F32) + 0.5 * rs_sum(pb2, f2, part, cols)
+            out[rows, cols] = (mixed[rows, cols].astype(F32) + 0.5 * rs_sum(pb2, f2, part, cols)).astype(BF)
 
     for name in ORDER:
         run_steps(name)
@@ -519,15 +553,14 @@
 
 
 def local(queries, keys, values, sink, stream, out_weight, norm_gain, gate_weight, up_weight, down_weight):
-    hbm = pl.BlockSpec(memory_space=pl.ANY)
+    hbm = pl.BlockSpec(memory_space=pltpu.HBM)
     vmem = pl.BlockSpec(memory_space=pltpu.VMEM)
-    smem = pl.BlockSpec(memory_space=pltpu.SMEM)
     V = pltpu.VMEM
     done = pl.pallas_call(
         kernel,
         name="layer",
-        out_shape=jax.ShapeDtypeStruct((BLK, D), F32),
-        in_specs=[hbm, hbm, hbm, smem, hbm, hbm, vmem, hbm, hbm, hbm, hbm],
+        out_shape=jax.ShapeDtypeStruct((BLK, D), BF),
+        in_specs=[hbm] * 11,
         out_specs=vmem,
         scratch_shapes=[
             V((NZ, NX, NC, ROWS, CA), BF),
@@ -552,7 +585,10 @@
             V((8, HALF, D), BF),
             V((2 * BLK, FFL), BF),
             V((FFL, D), BF),
-            pltpu.SemaphoreType.DMA((7,)),
+            V((CB // 256 + 1, BLK, 256), F32),
+            V((1, D), F32),
+            pltpu.SMEM((8,), F32),
+            pltpu.SemaphoreType.DMA((9,)),
             pltpu.SemaphoreType.DMA((NSEND,)),
             pltpu.SemaphoreType.DMA((NRECV,)),
         ],
@@ -563,7 +599,7 @@
         queries, keys, values, sink, stream, out_weight, norm_gain.reshape(1, D),
         gate_weight, up_weight, down_weight.T, jnp.asarray(tables()),
     )
-    return done.astype(BF)
+    return done
 
 
 def solution(mesh):

time: 90.4 us -> 89.1 us (0.986)
  other arithmetic: 2.24 us -> 0 us
  local copies, waits for them, and re-layouts: 0 us -> 1.98 us
  Pallas kernels: 88 us -> 87 us
    convert_element_type x1 -> x0, other arithmetic: 2.24 us -> none  [local(): return done.astype(BF)]
    unnamed x0 -> x1, local copies, waits for them, and re-layouts: none -> 1.98 us
    pallas_call x1, Pallas kernels: 88 us -> 87 us  [local(): pl.pallas_call(kernel, name='layer', out_shape=jax.ShapeDtypeStruct((BLK,...]
where the time goes in v4:
time: 89.1 us; the launch traced here: 89 us
  Pallas kernels  87 us (98%)
  local copies, waits for them, and re-layouts  1.98 us (2%)
    pallas_call x1, Pallas kernels, local(): pl.pallas_call(kernel, name='layer', out_shape=jax.ShapeDtypeStruct((BLK,...  87 us
    unnamed x1, local copies, waits for them, and re-layouts  1.98 us

profile of v4, /device:TPU:1, one launch (start us, length us, event | category | flops | bytes accessed | tf_op | source)
XLA Modules:
  0.0 89.0 jit_solution(7362311217426244954)
XLA Ops:
  0.0 87.0 %layer.1 = bf16[160,2048]{1,0:T(8,128)(2,1)} custom-call(bf16[640,512]{1,0:T(8,128)(2,1)} %q_hbm.1, bf16[640,128]{1,0:T(8,128)(2,1)} %k_hbm.1, bf16[640,128]{1,0:T(8,128)(2,1)} %v_hbm.1, f32[8]{0:T(128)} %sink_hbm.1, bf16[160,2048]{1,0:T(8,128)(2,1)} %st_hbm.1, bf16[512,2048]{1,0:T(8,128)(2,1)} %ow_hbm.1, f32[1,2048]{1,0:T(1,128)} %bitcast.3, ...), custom_call_target="tpu_custom_call" | custom-call | tf_op jit(solution)/shard_map/layer/pallas_call | solution.py:559
  87.0 2.0 %copy.13 = bf16[160,2048]{1,0:T(8,128)(2,1)} copy(bf16[160,2048]{1,0:T(8,128)(2,1)} %layer.1) | data formatting | bytes 1310720

commit v5 on v4

--- a/solution.py
+++ b/solution.py
@@ -25,18 +25,18 @@
 CB = 2 * GB
 CA = 2 * (FFL - GB) + FFL
 QW = 512
-NRECV = 63
+NRECV = 68
 NSEND = 14
 ORDER = (
     "begin", "turn_q", "prep_own", "prepare", "att_f", "proj_f", "bz_1", "att_n", "proj_n", "att_p", "az_1_0",
-    "proj_p", "ax_mid", "att_o", "rl-0", "proj_o", "bz_2", "bm_1", "rl+0", "bm_0", "az_2_0", "rl+1", "near+", "rl-1",
-    "bm_-1", "ax_end", "az_1_1", "tr_0", "az_1_-1", "bm_2", "bz_3", "norm_U", "bm_-2", "az_3_0", "be_1", "az_1_2",
-    "be_0", "tr_1", "tr_-1", "be_-1", "az_2_1", "norm_L", "be_2", "az_2_-1", "bz_4", "bm_3", "az_4_0", "az_2_2",
-    "gU", "bm_-3", "tr_2", "tr_-2", "az_3_1", "be_-2", "gL0", "az_3_-1", "bm_4", "az_3_2", "gL1", "early1", "az_4_1",
-    "be_3", "tr_3", "az_4_-1", "tr_-3", "be_-3", "az_4_2", "be_4", "tr_4", "feed1", "near0", "near1", "feed2",
-    "feed3", "r2l0", "r2l1", "fin0", "fin1",
+    "ax_mid", "proj_p", "att_o", "proj_o", "rl+0", "bm_1", "bz_2", "rl-0", "bm_0", "az_2_0", "rl+1", "near+", "rl-1",
+    "bm_-1", "ax_end", "az_1_1", "tr_0", "be_1", "az_1_-1", "bm_2", "bz_3", "norm_U", "az_3_0", "bm_-2", "az_1_2",
+    "be_0", "tr_1", "tr_-1", "be_-1", "az_2_1", "norm_L", "be_2", "az_2_-1", "bz_4", "bm_3", "az_4_0", "gU",
+    "az_2_2", "bm_-3", "tr_2", "tr_-2", "az_3_1", "be_-2", "gL0", "az_3_-1", "bm_4", "az_3_2", "gL1", "early1",
+    "tr_3", "be_3", "az_4_1", "tr_-3", "az_4_-1", "be_-3", "az_4_2", "early2", "be_4", "tr_4", "feed1", "near0",
+    "near1", "near2", "near3", "feed2", "feed3", "r2l0", "r2l1", "r2l2", "r2l3", "fin0", "fin1", "fin2", "fin3",
 )
-SUB = 2
+SUB = {"r1": 2, "r2": 4}
 
 
 def tables():
@@ -59,8 +59,8 @@
     q_hbm, k_hbm, v_hbm, sink_hbm, st_hbm, ow_hbm, gain_hbm, g_hbm, u_hbm, d_hbm, tab_hbm,
     out,
     wa, wb, tab, q, qr, kv, kk, vv, ow, st, bias, att,
-    pb1, s1, f1, pb2, s2, f2, mixed, xs, hid, dt, pre, gain, sink,
-    lsem, ssem, rsem,
+    pb1, s1, f1, pb2, s2, f2, mixed, xs, hid, dt, pre, gain, sink, res,
+    lsem, ssem, rsem, osem,
 ):
     s = lax.axis_index("sp")
     y = lax.axis_index("tp")
@@ -146,7 +146,7 @@
     way = ((1, 0), (-1, 1))
 
     def b_mate(dz, dx):
-        send(("bm", abs(dz) > 2), "bm", xb(dz, dx), mate)
+        send(("bm", max(abs(dz), 2)), "bm", xb(dz, dx), mate)
 
     def a_mate(dz, dx):
         send(("am", dz), "am", za(dz, dx), mate)
@@ -212,8 +212,8 @@
         recv(("am", dz), wa.at[0, :, 0])
         dt[:, pl.ds(pl.multiple_of(zz * 256, 256), 256)] = wa[zz, :, :, :, 2 * rest :].reshape(256, FFL).T
 
-    def mates(last):
-        recv(("bm", last), wb.at[pl.ds(0, 3 if last else 5), :, 0])
+    def mates(n):
+        recv(("bm", n), wb.at[pl.ds(0, {2: 5, 3: 2, 4: 1}[n]), :, 0])
 
     def begin():
         loaded("kv", kv.at[:, pl.ds(0, TOK)])
@@ -314,7 +314,8 @@
     ahead = {1: "n", -1: "p"}
     back = {1: "p", -1: "n"}
     via = {1: UP, -1: LOW}
-    cols_of = [pl.ds(i * (D // SUB), D // SUB) for i in range(SUB)]
+    cols_in = {tag: [pl.ds(i * (D // n), D // n) for i in range(n)] for tag, n in SUB.items()}
+    cols_of = cols_in["r1"]
 
     def project(block):
         def cols(n, carry):
@@ -327,7 +328,7 @@
         lax.fori_loop(0, 4, cols, 0)
 
     def rs_far(tag, pb, sbuf):
-        for i, cols in enumerate(cols_of):
+        for i, cols in enumerate(cols_in[tag]):
             for r in (1, -1):
                 key = (tag, "s", i) if tag == "r2" else (tag, "s", r, i)
                 send(key, tag, pb.at[at_half["f", via[r]], :, cols], ydev[r], sbuf.at[via[r], :, cols])
@@ -336,11 +337,11 @@
         return (tag, "f", i if tag == "r2" else part)
 
     def rs_near(tag, pb, fbuf, r, i):
-        part, cols = 1 - via[r], cols_of[i]
+        part, cols = 1 - via[r], cols_in[tag][i]
         send(sum_key(tag, part, i), tag, pb.at[at_half[ahead[r], part], :, cols], ydev[r], fbuf.at[part, via[r], :, cols])
 
     def rs_relay(tag, pb, sbuf, fbuf, r, i):
-        cols, part = cols_of[i], via[r]
+        cols, part = cols_in[tag][i], via[r]
         j = at_half[ahead[r], part]
         if tag == "r1":
             recv((tag, "s", r, i), sbuf.at[part, :, cols])
@@ -410,19 +411,24 @@
         return mm(act, w.reshape(256, 256))
 
     def early():
-        mates(False)
+        mates(2)
         for n in range(CB // 256 + 1):
             acc = over(n, 0)
             for dz in (1, -1, 2, -2):
                 acc = acc + over(n, dz)
             pre[n] = acc
 
+    def early_more():
+        mates(3)
+        for n in range(CB // 256 + 1):
+            pre[n] = pre[n] + over(n, 3) + over(n, -3)
+
     def late():
-        mates(True)
+        mates(4)
         parts_of = GB // 256
 
         def total(n):
-            return pre[n] + over(n, 3) + over(n, -3) + over(n, 4)
+            return pre[n] + over(n, 4)
 
         def act(gate, upward):
             return (gate / (1.0 + jnp.exp(-gate)) * upward).astype(BF)
@@ -436,12 +442,12 @@
         many = count * HALF
 
         def cols(n, carry):
-            at_n = pl.ds(pl.multiple_of(i * (D // SUB) + n * 512, 512), 512)
+            at_n = pl.ds(pl.multiple_of(i * (D // SUB["r2"]) + n * 512, 512), 512)
             done = mm(hid[pl.ds(0, many), :], dt[:, at_n]).astype(BF)
             pb2[first : first + count, :, at_n] = done.reshape(count, HALF, 512)
             return carry
 
-        lax.fori_loop(0, D // SUB // 512, cols, 0, unroll=True)
+        lax.fori_loop(0, D // SUB["r2"] // 512, cols, 0, unroll=True)
 
     def near2(i):
         down(0, 2, i)
@@ -451,21 +457,21 @@
     def far2():
         g_far()
         gate_up(2, 2)
-        for i in range(SUB):
+        for i in range(SUB["r2"]):
             down(2, 2, i)
         rs_far("r2", pb2, s2)
 
     def own2():
         gate_up(4, 4)
-        for i in range(SUB):
+        for i in range(SUB["r2"]):
             down(4, 4, i)
 
     def near1(r):
-        for i in range(SUB):
+        for i in range(SUB["r1"]):
             rs_near("r1", pb1, f1, r, i)
 
     def relay2(i):
-        recv(("r2", "s", i), s2.at[:, :, cols_of[i]])
+        recv(("r2", "s", i), s2.at[:, :, cols_in["r2"][i]])
         for r in (1, -1):
             rs_relay("r2", pb2, s2, f2, r, i)
 
@@ -505,19 +511,16 @@
         "ax_end": ax_end,
         "early1": early,
         "feed1": late,
-        "near0": lambda: near2(0),
-        "near1": lambda: near2(1),
+        "early2": early_more,
         "feed2": far2,
         "feed3": own2,
-        "r2l0": lambda: relay2(0),
-        "r2l1": lambda: relay2(1),
-        "fin0": lambda: finish(0),
-        "fin1": lambda: finish(1),
     }
 
     def run_steps(name):
         if name in steps:
             return steps[name]()
+        if name[:-1] in ("near", "r2l", "fin"):
+            return {"near": near2, "r2l": relay2, "fin": finish}[name[:-1]](int(name[-1]))
         head, *rest_of = name.split("_")
         if head == "att":
             return attend_on(rest_of[0])
@@ -529,11 +532,12 @@
         return {"bz": bz, "bm": bx_mid, "be": bx_end, "az": az, "tr": turn_down}[head](*numbers)
 
     def finish(i):
-        cols = cols_of[i]
-        recv(("r2", "f", i), pb2.at[pl.ds(0, 2)])
+        cols = cols_in["r2"][i]
+        recv(("r2", "f", i), pb2.at[pl.ds(0, 4), :, cols])
         for part in (UP, LOW):
             rows = pl.ds(part * HALF, HALF)
-            out[rows, cols] = (mixed[rows, cols].astype(F32) + 0.5 * rs_sum(pb2, f2, part, cols)).astype(BF)
+            res[rows, cols] = (mixed[rows, cols].astype(F32) + 0.5 * rs_sum(pb2, f2, part, cols)).astype(BF)
+        pltpu.make_async_copy(res.at[:, cols], out.at[:, cols], osem).start()
 
     for name in ORDER:
         run_steps(name)
@@ -549,19 +553,19 @@
             pltpu.make_async_copy(ref, ref, ssem.at[given[kind]]).wait()
 
     drain()
+    pltpu.make_async_copy(res, out, osem).wait()
     assert len(taken) == NRECV and len(given) == NSEND, (len(taken), len(given))
 
 
 def local(queries, keys, values, sink, stream, out_weight, norm_gain, gate_weight, up_weight, down_weight):
     hbm = pl.BlockSpec(memory_space=pltpu.HBM)
-    vmem = pl.BlockSpec(memory_space=pltpu.VMEM)
     V = pltpu.VMEM
     done = pl.pallas_call(
         kernel,
         name="layer",
         out_shape=jax.ShapeDtypeStruct((BLK, D), BF),
         in_specs=[hbm] * 11,
-        out_specs=vmem,
+        out_specs=hbm,
         scratch_shapes=[
             V((NZ, NX, NC, ROWS, CA), BF),
             V((NZ, NX, NC, ROWS, CB), BF),
@@ -588,9 +592,11 @@
             V((CB // 256 + 1, BLK, 256), F32),
             V((1, D), F32),
             pltpu.SMEM((8,), F32),
+            V((BLK, D), BF),
             pltpu.SemaphoreType.DMA((9,)),
             pltpu.SemaphoreType.DMA((NSEND,)),
             pltpu.SemaphoreType.DMA((NRECV,)),
+            pltpu.SemaphoreType.DMA,
         ],
         compiler_params=pltpu.CompilerParams(
             collective_id=0, has_side_effects=True, vmem_limit_bytes=62 * 1024 * 1024

time: 89.1 us -> 88.5 us (level)
  no operation moved by 1% of the time
where the time goes in v5:
time: 88.5 us; the launch traced here: 88.3 us
  Pallas kernels  86.3 us (98%)
  local copies, waits for them, and re-layouts  1.98 us (2%)
    pallas_call x1, Pallas kernels, local(): pl.pallas_call(kernel, name='layer', out_shape=jax.ShapeDtypeStruct((BLK,...  86.3 us
    unnamed x1, local copies, waits for them, and re-layouts  1.98 us

profile of v5, /device:TPU:1, one launch (start us, length us, event | category | flops | bytes accessed | tf_op | source)
XLA Modules:
  0.0 88.3 jit_solution(10094519241185988597)
XLA Ops:
  0.0 86.3 %layer.1 = bf16[160,2048]{1,0:T(8,128)(2,1)} custom-call(bf16[640,512]{1,0:T(8,128)(2,1)} %q_hbm.1, bf16[640,128]{1,0:T(8,128)(2,1)} %k_hbm.1, bf16[640,128]{1,0:T(8,128)(2,1)} %v_hbm.1, f32[8]{0:T(128)} %sink_hbm.1, bf16[160,2048]{1,0:T(8,128)(2,1)} %st_hbm.1, bf16[512,2048]{1,0:T(8,128)(2,1)} %ow_hbm.1, f32[1,2048]{1,0:T(1,128)} %bitcast.3, ...), custom_call_target="tpu_custom_call" | custom-call | tf_op jit(solution)/shard_map/layer/pallas_call | solution.py:563
  86.4 2.0 %copy.13 = bf16[160,2048]{1,0:T(8,128)(2,1)} copy(bf16[160,2048]{1,0:T(8,128)(2,1)} %layer.1) | data formatting | bytes 1310720

commit v6 on v5

--- a/solution.py
+++ b/solution.py
@@ -26,7 +26,7 @@
 CA = 2 * (FFL - GB) + FFL
 QW = 512
 NRECV = 68
-NSEND = 14
+NSEND = 8
 ORDER = (
     "begin", "turn_q", "prep_own", "prepare", "att_f", "proj_f", "bz_1", "att_n", "proj_n", "att_p", "az_1_0",
     "ax_mid", "proj_p", "att_o", "proj_o", "rl+0", "bm_1", "bz_2", "rl-0", "bm_0", "az_2_0", "rl+1", "near+", "rl-1",
@@ -146,10 +146,10 @@
     way = ((1, 0), (-1, 1))
 
     def b_mate(dz, dx):
-        send(("bm", max(abs(dz), 2)), "bm", xb(dz, dx), mate)
+        send(("bm", max(abs(dz), 2)), "bx", xb(dz, dx), mate)
 
     def a_mate(dz, dx):
-        send(("am", dz), "am", za(dz, dx), mate)
+        send(("am", dz), "az", za(dz, dx), mate)
 
     def bx_send(dz):
         for r in (1, -1):
@@ -159,7 +159,7 @@
     def bx_mid(dz):
         recv(("bx", dz), twob)
         for r, half in way:
-            send(("bh", dz), "bh", xb(dz, -r, half), xdev[r])
+            send(("bh", dz), "bz", xb(dz, -r, half), xdev[r])
         for r in (1, -1):
             b_mate(dz, r)
 
@@ -173,7 +173,7 @@
             if n < 3:
                 send(("bz", n + 1), "bz", zb(-r * n), zdev[r])
             elif n == 3:
-                send(("bz", 4), "bzh", zb(-r * 3, half), zdev[r])
+                send(("bz", 4), "bz", zb(-r * 3, half), zdev[r])
         for dz in (n, -n) if n < 4 else (4,):
             bx_send(dz)
 
@@ -181,7 +181,7 @@
         if n < 4:
             send(("az", n, dx), "az", za(-r * (n - 1), dx), zdev[r])
         else:
-            send(("az", 4, dx), "azh", za(-r * 3, dx, 0 if r == 1 else 1), zdev[r])
+            send(("az", 4, dx), "ax", za(-r * 3, dx, 0 if r == 1 else 1), zdev[r])
 
     def az(n, dx):
         recv(("az", n, dx), twoa if n < 4 else onea)
@@ -194,7 +194,7 @@
     def ax_mid():
         recv(("ax",), twoa)
         for r, half in way:
-            send(("ah",), "ah", xa(-r, half), xdev[r])
+            send(("ah",), "ax", xa(-r, half), xdev[r])
         for r in (1, -1):
             for dx in (1, -1):
                 az_send(1, dx, r)
@@ -325,7 +325,7 @@
                 pb1[at_half[block, part], :, at_n] = done[part * HALF : (part + 1) * HALF]
             return carry
 
-        lax.fori_loop(0, 4, cols, 0)
+        lax.fori_loop(0, 4, cols, 0, unroll=True)
 
     def rs_far(tag, pb, sbuf):
         for i, cols in enumerate(cols_in[tag]):
@@ -545,9 +545,9 @@
     def drain():
         everything = {
             "halo": kv.at[:, pl.ds(0, 2 * WINDOW)],
-            "bz": wb.at[pl.ds(0, 6), 0, 0], "bzh": oneb, "bx": wb.at[:, pl.ds(0, 2), 0], "bh": wb.at[:, 0, 0],
-            "bm": wb.at[:, :, 0], "ax": twoa, "ah": onea, "az": wa.at[pl.ds(0, 6), :, 0], "azh": wa.at[0, :, 0],
-            "am": wa.at[:, :, 0], "r1": pb1.at[pl.ds(0, 6)], "r2": pb2.at[pl.ds(0, 6)], "g": xs.at[pl.ds(0, 6)],
+            "bz": wb.at[pl.ds(0, 5), pl.ds(0, 3), 0], "bx": wb.at[pl.ds(0, 6)],
+            "ax": wa.at[pl.ds(0, 7), 0, 0], "az": wa.at[pl.ds(0, 7)],
+            "r1": pb1.at[pl.ds(0, 6)], "r2": pb2.at[pl.ds(0, 6)], "g": xs.at[pl.ds(0, 6)],
         }
         for kind, ref in everything.items():
             pltpu.make_async_copy(ref, ref, ssem.at[given[kind]]).wait()
@@ -605,7 +605,29 @@
         queries, keys, values, sink, stream, out_weight, norm_gain.reshape(1, D),
         gate_weight, up_weight, down_weight.T, jnp.asarray(tables()),
     )
-    return done
+    half = BLK // 2
+
+    def copy_out(src, dst, held, sems):
+        for way in range(2):
+            for i in range(2):
+                rows = pl.ds(i * half, half)
+                if way:
+                    pltpu.make_async_copy(src.at[rows], held.at[rows], sems.at[0, i]).wait()
+                    pltpu.make_async_copy(held.at[rows], dst.at[rows], sems.at[1, i]).start()
+                else:
+                    pltpu.make_async_copy(src.at[rows], held.at[rows], sems.at[0, i]).start()
+        for i in range(2):
+            rows = pl.ds(i * half, half)
+            pltpu.make_async_copy(held.at[rows], dst.at[rows], sems.at[1, i]).wait()
+
+    return pl.pallas_call(
+        copy_out,
+        name="copy_out",
+        out_shape=jax.ShapeDtypeStruct((BLK, D), BF),
+        in_specs=[hbm],
+        out_specs=hbm,
+        scratch_shapes=[V((BLK, D), BF), pltpu.SemaphoreType.DMA((2, 2))],
+    )(done)
 
 
 def solution(mesh):

time: 88.5 us -> 87.5 us (0.989)
  local copies, waits for them, and re-layouts: 1.98 us -> 0 us
  Pallas kernels: 86.3 us -> 87.2 us
    unnamed x1 -> x0, local copies, waits for them, and re-layouts: 1.98 us -> none
    pallas_call x0 -> x1, Pallas kernels: none -> 1.84 us  [local(): pl.pallas_call(copy_out, name='copy_out', out_shape=jax.ShapeDtypeStruct(...]
    pallas_call x1, Pallas kernels: 86.3 us -> 85.4 us  [local(): pl.pallas_call(kernel, name='layer', out_shape=jax.ShapeDtypeStruct((BLK,...]
where the time goes in v6:
time: 87.5 us; the launch traced here: 87.4 us
  Pallas kernels  87.2 us (100%)
    pallas_call x1, Pallas kernels, local(): pl.pallas_call(kernel, name='layer', out_shape=jax.ShapeDtypeStruct((BLK,...  85.4 us
    pallas_call x1, Pallas kernels, local(): pl.pallas_call(copy_out, name='copy_out', out_shape=jax.ShapeDtypeStruct(...  1.84 us

profile of v6, /device:TPU:1, one launch (start us, length us, event | category | flops | bytes accessed | tf_op | source)
XLA Modules:
  0.0 87.4 jit_solution(1327267940272298365)
XLA Ops:
  0.0 85.4 %layer.1.src = bf16[160,2048]{1,0:T(8,128)(2,1)} custom-call(bf16[640,512]{1,0:T(8,128)(2,1)} %q_hbm.1, bf16[640,128]{1,0:T(8,128)(2,1)} %k_hbm.1, bf16[640,128]{1,0:T(8,128)(2,1)} %v_hbm.1, f32[8]{0:T(128)} %sink_hbm.1, bf16[160,2048]{1,0:T(8,128)(2,1)} %st_hbm.1, bf16[512,2048]{1,0:T(8,128)(2,1)} %ow_hbm.1, f32[1,2048]{1,0:T(1,128)} %bitcast.3, ...), custom_call_target="tpu_custom_call" | custom-call | tf_op jit(solution)/shard_map/layer/pallas_call | solution.py:563
  85.4 1.8 %copy_out.1 = bf16[160,2048]{1,0:T(8,128)(2,1)} custom-call(bf16[160,2048]{1,0:T(8,128)(2,1)} %layer.1.src), custom_call_target="tpu_custom_call" | custom-call | tf_op jit(solution)/shard_map/copy_out/pallas_call | solution.py:623
